TPU v7x, 512 devices: a whole 4x8x8 slice. The times are simulated.
512 devices in a mesh: sp: 64 (over z, y), tp: 8 (over x, core).
Axes of the slice: x: 4, y: 8, z: 8, core: 2. Of those that a mesh axis runs over, the one named last changes fastest.
Arguments:
- resid: bfloat16 [16384, 2048], P(('sp', 'tp')), may hold values from -6 to 6
- queries: bfloat16 [16384, 2048], P('sp', 'tp'), may hold values from -6 to 6
- keys: bfloat16 [16384, 1024], P('sp', 'tp'), may hold values from -6 to 6
- values: bfloat16 [16384, 1024], P('sp', 'tp'), may hold values from -6 to 6
- log_gates: float32 [16, 16384], P('tp'), as said below
- documents: int32 [16384], P('sp'), may hold values from 0 to 2, never falling along the last dimension, each value on 1 to 12288 neighbouring positions
- out_weight: bfloat16 [2048, 2048], P('tp'), may hold values from -0.125 to 0.125
- attn_gain: float32 [2048], replicated, may hold values from 0.1 to 1.9
- mlp_gain: float32 [2048], replicated, may hold values from 0.1 to 1.9
- gate_weight: bfloat16 [2048, 4096], P('sp', 'tp'), may hold values from -0.125 to 0.125
- up_weight: bfloat16 [2048, 4096], P('sp', 'tp'), may hold values from -0.125 to 0.125
- down_weight: bfloat16 [4096, 2048], P('tp', 'sp'), may hold values from -0.375 to 0.375
Outputs:
- mixed: bfloat16 [16384, 2048], P(('sp', 'tp'))
Inputs may be any that keep to these rules, and one draw needn't show every extreme that they name: `log_gates`: each head's row never rises from one position to the next and starts at or below 0. `documents`: document numbers never fall along the positions; one document spans exactly three quarters of the 16384 positions.
All inputs are finite; a program needn't handle non-finite values.
Results may differ from a plain program's by a relative error of at most 0.018.
Values may be sent and summed in bfloat16 or wider, within the bound.
A program may use at most 64 MiB of HBM per device.

v0:
```python
import math

import jax
import jax.numpy as jnp
from jax import lax
from jax.sharding import PartitionSpec as P

HD = 128


def turned_gather(arrays, axis, dims):
    turned = [jnp.moveaxis(a, dim, 0) for a, dim in zip(arrays, dims)]
    widths = [t[0].size for t in turned]
    both = jnp.concatenate([t.reshape(-1, w) for t, w in zip(turned, widths)], axis=1)
    filled = lax.all_gather(both, axis, axis=0, tiled=True)
    blocks = jnp.split(filled, [sum(widths[:k]) for k in range(1, len(widths))], axis=1)
    return tuple(
        (
            jnp.moveaxis(b.reshape(-1, *t.shape[1:]), 0, dim)
            for b, t, dim in zip(blocks, turned, dims)
        )
    )


def side_by_side(arrays, axis, dim, along):
    ends, at = ([], 0)
    for a in arrays[:-1]:
        at += a.shape[along]
        ends.append(at)
    both = jnp.concatenate(arrays, axis=along)
    return tuple(jnp.split(lax.all_gather(both, axis, axis=dim, tiled=True), ends, axis=along))


def split_up(array, dim, size):
    before, after = (array.shape[:dim], array.shape[dim + 1 :])
    return jnp.moveaxis(array.reshape(*before, size, -1, *after), dim, 0)


def sent_and_summed(array, axis, dim):
    blocks = split_up(array, dim, lax.axis_size(axis))
    arrived = lax.all_to_all(blocks, axis, split_axis=0, concat_axis=0, tiled=True)
    return arrived.astype(jnp.float32).sum(axis=0)


def joined_along(blocks, dim):
    blocks = jnp.moveaxis(blocks, 0, dim)
    dims = blocks.shape
    return blocks.reshape(*dims[:dim], dims[dim] * dims[dim + 1], *dims[dim + 2 :])


def sent_to_all(array, axis):
    size = lax.axis_size(axis)
    return lax.all_to_all(
        jnp.broadcast_to(array[None], (size, *array.shape)), axis, 0, 0, tiled=True
    )


def gather_directly(array, axis, dim):
    return joined_along(sent_to_all(array, axis), dim)


def local(
    resid,
    queries,
    keys,
    values,
    log_gates,
    documents,
    out_weight,
    attn_gain,
    mlp_gain,
    gate_weight,
    up_weight,
    down_weight,
):
    tok_rows = queries.shape[0]
    kv_dev = keys.shape[1] // HD
    heads_dev = log_gates.shape[0]
    group_size = heads_dev // kv_dev
    score_scale = 1.0 / math.sqrt(HD)
    own_start = lax.axis_index("sp") * tok_rows
    own_last = own_start + tok_rows - 1
    first_doc = documents[0]
    query_pos = own_start + lax.iota(jnp.int32, tok_rows)
    query_heads = queries.reshape(tok_rows, kv_dev, group_size, HD)
    key_gates_all = log_gates.reshape(kv_dev, group_size, log_gates.shape[1])
    query_gates = lax.dynamic_slice_in_dim(key_gates_all, own_start, tok_rows, 2)
    collected = turned_gather((gate_weight, up_weight, down_weight), "sp", (0, 0, 1))
    residual_rows = resid.astype(jnp.float32)

    def attend_block(running, key_rows, value_rows, doc_rows, first_row):
        run_max, run_sum, accumulated = running
        key_count = key_rows.shape[0]
        scores = (
            jnp.einsum(
                "tkgd,skd->kgts",
                query_heads,
                key_rows.reshape(key_count, kv_dev, HD),
                preferred_element_type=jnp.float32,
            )
            * score_scale
        )
        key_gates = lax.dynamic_slice_in_dim(key_gates_all, first_row, key_count, 2)
        scores = scores + query_gates[..., None] - key_gates[:, :, None, :]
        key_pos = first_row + lax.iota(jnp.int32, key_count)
        visible = (key_pos[None, :] <= query_pos[:, None]) & (
            doc_rows[None, :] == documents[:, None]
        )
        scores = jnp.where(visible, scores, jnp.float32(-1e30))
        new_max = jnp.maximum(run_max, jnp.max(scores, axis=-1))
        probs = jnp.where(visible, jnp.exp(scores - new_max[..., None]), jnp.float32(0.0))
        shrink = jnp.exp(run_max - new_max)
        run_sum = run_sum * shrink + jnp.sum(probs, axis=-1)
        weighted = jnp.einsum(
            "kgts,skd->kgtd",
            probs.astype(jnp.bfloat16),
            value_rows.reshape(key_count, kv_dev, HD),
            preferred_element_type=jnp.float32,
        )
        accumulated = accumulated * shrink[..., None] + weighted
        return (new_max, run_sum, accumulated)

    def maybe_attend(running, key_rows, value_rows, doc_rows, first_row):
        needed = (first_row <= own_last) & (doc_rows[-1] >= first_doc)

        def compute(state):
            return attend_block(state, key_rows, value_rows, doc_rows, first_row)

        def keep(state):
            return state

        return lax.cond(needed, compute, keep, running)

    start_state = (
        jnp.full((kv_dev, group_size, tok_rows), -1e30, jnp.float32),
        jnp.zeros((kv_dev, group_size, tok_rows), jnp.float32),
        jnp.zeros((kv_dev, group_size, tok_rows, HD), jnp.float32),
    )
    key_rows, value_rows, doc_rows = (
        *side_by_side((keys, values), "sp", 0, 1),
        lax.all_gather(documents, "sp", axis=0, tiled=True),
    )
    key_count = key_rows.shape[0]
    block_len = math.gcd(key_count, 1024)

    def advance(block_index, inner):
        offset = block_index * block_len
        return maybe_attend(
            inner,
            lax.dynamic_slice_in_dim(key_rows, offset, block_len, 0),
            lax.dynamic_slice_in_dim(value_rows, offset, block_len, 0),
            lax.dynamic_slice_in_dim(doc_rows, offset, block_len, 0),
            offset,
        )

    run_max, run_sum, accumulated = lax.fori_loop(0, key_count // block_len, advance, start_state)
    attended = accumulated / run_sum[..., None]
    attended = (
        jnp.transpose(attended, (2, 0, 1, 3)).reshape(tok_rows, heads_dev * HD).astype(jnp.bfloat16)
    )
    rows_slice = attended
    projected = sent_and_summed(
        jnp.dot(rows_slice, out_weight, preferred_element_type=jnp.float32).astype(jnp.bfloat16),
        "tp",
        0,
    )
    power = jnp.mean(projected * projected, axis=-1, keepdims=True)
    middle = residual_rows + attn_gain * projected * lax.rsqrt(power + 1e-06)
    middle_power = jnp.mean(middle * middle, axis=-1, keepdims=True)
    normed = (mlp_gain * middle * lax.rsqrt(middle_power + 1e-06)).astype(jnp.bfloat16)
    normed_all = gather_directly(normed, "tp", 0)
    gate_full, up_full, down_full = collected
    gate_act = jnp.dot(normed_all, gate_full, preferred_element_type=jnp.float32)
    up_act = jnp.dot(normed_all, up_full, preferred_element_type=jnp.float32)
    hidden = (jax.nn.silu(gate_act) * up_act).astype(jnp.bfloat16)
    rows_slice = hidden
    lowered = sent_and_summed(
        jnp.dot(rows_slice, down_full, preferred_element_type=jnp.float32).astype(jnp.bfloat16),
        "tp",
        0,
    )
    return (middle + 0.5 * lowered).astype(jnp.bfloat16)


def solution(mesh):
    placed = (
        P(("sp", "tp"), None),
        P("sp", "tp"),
        P("sp", "tp"),
        P("sp", "tp"),
        P("tp", None),
        P("sp"),
        P("tp", None),
        P(),
        P(),
        P("sp", "tp"),
        P("sp", "tp"),
        P("tp", "sp"),
    )
    return jax.shard_map(
        local, mesh=mesh, in_specs=placed, out_specs=P(("sp", "tp"), None), check_vma=False
    )
```

profile of v0, /device:TPU:368, one launch (start us, length us, event | category | flops | bytes accessed | tf_op | source)
XLA Modules:
  0.0 276.5 jit_solution(11792429158907779249)
XLA Ops:
  12.1 46.2 %all-gather = s32[64,1,256]{2,1,0:T(1,128)S(1)} all-gather(s32[1,1,256]{2,1,0:T(1,128)} %bitcast.71), channel_id=1, replica_groups=mesh['sp'=64,'tp'=8] {'sp'}, dimensions={0}, use_global_device_ids=true | all-gather | bytes 66560 | tf_op jit(solution)/shard_map/all_gather | solution.py:141
  59.0 48.5 %all-gather.4.cloned.1.call-done = bf16[16384,256]{1,0:T(8,128)(2,1)} async-done(((bf16[256,256]{1,0:T(8,128)(2,1)}), bf16[16384,256]{1,0:T(8,128)(2,1)}) %all-gather.4.cloned.1.call-update) | async-done | bytes 8388624 | tf_op jit(solution)/shard_map/all_gather | solution.py:31
  107.4 5.7 %fusion.42 = (bf16[16384,128]{1,0:T(8,128)(2,1)}, bf16[16384,128]{1,0:T(8,128)(2,1)}) fusion(bf16[16384,256]{1,0:T(8,128)(2,1)} %all-gather.4.cloned.1.call-done), kind=kLoop, calls=%fused_computation.59 | loop fusion | bytes 16777216 | tf_op jit(solution)/shard_map/split | solution.py:31
  113.2 88.2 %while.18 = (s32[]{:T(128)}, f32[1,2,256]{2,1,0:T(2,128)S(1)}, f32[1,2,256]{2,1,0:T(2,128)S(1)}, f32[1,2,256,128]{3,2,1,0:T(8,128)S(1)}, s32[]{:T(128)}, /*index...) while((s32[]{:T(128)}, f32[1,2,256]{2,1,0:T(2,128)S(1)}, ...), condition=%wide.region_5.6_spmd.clone, body=%wide.region_0.5_spmd.clone.sunk | while | flops 275122944 | bytes 8606159 | solution.py:156
  115.1 4.8 %conditional.3 = ((f32[1,2,256]{2,1,0:T(2,128)S(1)}, f32[1,2,256]{2,1,0:T(2,128)S(1)}, f32[1,2,256,128]{3,2,1,0:T(8,128)S(1)})) conditional(s32[]{:T(128)} %convert_element_type.79, (f32[1,2,256]{2,1,0:T(2,128)S(1)}, f32[1,2,256]{2,1,0:T(2,128)S(1)}, f32[1,2,256,128]{3,2,1,0:T(8,128)S(1)}) %tuple.51, (s32[]{:T(128)}, s32[]{:T(128)}, ...), branch_computations={%region_1.0_spmd, %region_2.4_spmd} | conditional | flops 275122944 | bytes 8596558 | solution.py:132
  121.8 4.8 %conditional.3 = ((f32[1,2,256]{2,1,0:T(2,128)S(1)}, f32[1,2,256]{2,1,0:T(2,128)S(1)}, f32[1,2,256,128]{3,2,1,0:T(8,128)S(1)})) conditional(s32[]{:T(128)} %convert_element_type.79, (f32[1,2,256]{2,1,0:T(2,128)S(1)}, f32[1,2,256]{2,1,0:T(2,128)S(1)}, f32[1,2,256,128]{3,2,1,0:T(8,128)S(1)}) %tuple.51, (s32[]{:T(128)}, s32[]{:T(128)}, ...), branch_computations={%region_1.0_spmd, %region_2.4_spmd} | conditional | flops 275122944 | bytes 8596558 | solution.py:132
  128.5 4.8 %conditional.3 = ((f32[1,2,256]{2,1,0:T(2,128)S(1)}, f32[1,2,256]{2,1,0:T(2,128)S(1)}, f32[1,2,256,128]{3,2,1,0:T(8,128)S(1)})) conditional(s32[]{:T(128)} %convert_element_type.79, (f32[1,2,256]{2,1,0:T(2,128)S(1)}, f32[1,2,256]{2,1,0:T(2,128)S(1)}, f32[1,2,256,128]{3,2,1,0:T(8,128)S(1)}) %tuple.51, (s32[]{:T(128)}, s32[]{:T(128)}, ...), branch_computations={%region_1.0_spmd, %region_2.4_spmd} | conditional | flops 275122944 | bytes 8596558 | solution.py:132
  135.2 4.8 %conditional.3 = ((f32[1,2,256]{2,1,0:T(2,128)S(1)}, f32[1,2,256]{2,1,0:T(2,128)S(1)}, f32[1,2,256,128]{3,2,1,0:T(8,128)S(1)})) conditional(s32[]{:T(128)} %convert_element_type.79, (f32[1,2,256]{2,1,0:T(2,128)S(1)}, f32[1,2,256]{2,1,0:T(2,128)S(1)}, f32[1,2,256,128]{3,2,1,0:T(8,128)S(1)}) %tuple.51, (s32[]{:T(128)}, s32[]{:T(128)}, ...), branch_computations={%region_1.0_spmd, %region_2.4_spmd} | conditional | flops 275122944 | bytes 8596558 | solution.py:132
  141.9 4.8 %conditional.3 = ((f32[1,2,256]{2,1,0:T(2,128)S(1)}, f32[1,2,256]{2,1,0:T(2,128)S(1)}, f32[1,2,256,128]{3,2,1,0:T(8,128)S(1)})) conditional(s32[]{:T(128)} %convert_element_type.79, (f32[1,2,256]{2,1,0:T(2,128)S(1)}, f32[1,2,256]{2,1,0:T(2,128)S(1)}, f32[1,2,256,128]{3,2,1,0:T(8,128)S(1)}) %tuple.51, (s32[]{:T(128)}, s32[]{:T(128)}, ...), branch_computations={%region_1.0_spmd, %region_2.4_spmd} | conditional | flops 275122944 | bytes 8596558 | solution.py:132
  148.6 4.8 %conditional.3 = ((f32[1,2,256]{2,1,0:T(2,128)S(1)}, f32[1,2,256]{2,1,0:T(2,128)S(1)}, f32[1,2,256,128]{3,2,1,0:T(8,128)S(1)})) conditional(s32[]{:T(128)} %convert_element_type.79, (f32[1,2,256]{2,1,0:T(2,128)S(1)}, f32[1,2,256]{2,1,0:T(2,128)S(1)}, f32[1,2,256,128]{3,2,1,0:T(8,128)S(1)}) %tuple.51, (s32[]{:T(128)}, s32[]{:T(128)}, ...), branch_computations={%region_1.0_spmd, %region_2.4_spmd} | conditional | flops 275122944 | bytes 8596558 | solution.py:132
  155.3 4.8 %conditional.3 = ((f32[1,2,256]{2,1,0:T(2,128)S(1)}, f32[1,2,256]{2,1,0:T(2,128)S(1)}, f32[1,2,256,128]{3,2,1,0:T(8,128)S(1)})) conditional(s32[]{:T(128)} %convert_element_type.79, (f32[1,2,256]{2,1,0:T(2,128)S(1)}, f32[1,2,256]{2,1,0:T(2,128)S(1)}, f32[1,2,256,128]{3,2,1,0:T(8,128)S(1)}) %tuple.51, (s32[]{:T(128)}, s32[]{:T(128)}, ...), branch_computations={%region_1.0_spmd, %region_2.4_spmd} | conditional | flops 275122944 | bytes 8596558 | solution.py:132
  162.0 4.8 %conditional.3 = ((f32[1,2,256]{2,1,0:T(2,128)S(1)}, f32[1,2,256]{2,1,0:T(2,128)S(1)}, f32[1,2,256,128]{3,2,1,0:T(8,128)S(1)})) conditional(s32[]{:T(128)} %convert_element_type.79, (f32[1,2,256]{2,1,0:T(2,128)S(1)}, f32[1,2,256]{2,1,0:T(2,128)S(1)}, f32[1,2,256,128]{3,2,1,0:T(8,128)S(1)}) %tuple.51, (s32[]{:T(128)}, s32[]{:T(128)}, ...), branch_computations={%region_1.0_spmd, %region_2.4_spmd} | conditional | flops 275122944 | bytes 8596558 | solution.py:132
  168.7 4.8 %conditional.3 = ((f32[1,2,256]{2,1,0:T(2,128)S(1)}, f32[1,2,256]{2,1,0:T(2,128)S(1)}, f32[1,2,256,128]{3,2,1,0:T(8,128)S(1)})) conditional(s32[]{:T(128)} %convert_element_type.79, (f32[1,2,256]{2,1,0:T(2,128)S(1)}, f32[1,2,256]{2,1,0:T(2,128)S(1)}, f32[1,2,256,128]{3,2,1,0:T(8,128)S(1)}) %tuple.51, (s32[]{:T(128)}, s32[]{:T(128)}, ...), branch_computations={%region_1.0_spmd, %region_2.4_spmd} | conditional | flops 275122944 | bytes 8596558 | solution.py:132
  171.4 1.7 fusion.6
  175.5 4.8 %conditional.3 = ((f32[1,2,256]{2,1,0:T(2,128)S(1)}, f32[1,2,256]{2,1,0:T(2,128)S(1)}, f32[1,2,256,128]{3,2,1,0:T(8,128)S(1)})) conditional(s32[]{:T(128)} %convert_element_type.79, (f32[1,2,256]{2,1,0:T(2,128)S(1)}, f32[1,2,256]{2,1,0:T(2,128)S(1)}, f32[1,2,256,128]{3,2,1,0:T(8,128)S(1)}) %tuple.51, (s32[]{:T(128)}, s32[]{:T(128)}, ...), branch_computations={%region_1.0_spmd, %region_2.4_spmd} | conditional | flops 275122944 | bytes 8596558 | solution.py:132
  182.2 4.8 %conditional.3 = ((f32[1,2,256]{2,1,0:T(2,128)S(1)}, f32[1,2,256]{2,1,0:T(2,128)S(1)}, f32[1,2,256,128]{3,2,1,0:T(8,128)S(1)})) conditional(s32[]{:T(128)} %convert_element_type.79, (f32[1,2,256]{2,1,0:T(2,128)S(1)}, f32[1,2,256]{2,1,0:T(2,128)S(1)}, f32[1,2,256,128]{3,2,1,0:T(8,128)S(1)}) %tuple.51, (s32[]{:T(128)}, s32[]{:T(128)}, ...), branch_computations={%region_1.0_spmd, %region_2.4_spmd} | conditional | flops 275122944 | bytes 8596558 | solution.py:132
  188.9 4.8 %conditional.3 = ((f32[1,2,256]{2,1,0:T(2,128)S(1)}, f32[1,2,256]{2,1,0:T(2,128)S(1)}, f32[1,2,256,128]{3,2,1,0:T(8,128)S(1)})) conditional(s32[]{:T(128)} %convert_element_type.79, (f32[1,2,256]{2,1,0:T(2,128)S(1)}, f32[1,2,256]{2,1,0:T(2,128)S(1)}, f32[1,2,256,128]{3,2,1,0:T(8,128)S(1)}) %tuple.51, (s32[]{:T(128)}, s32[]{:T(128)}, ...), branch_computations={%region_1.0_spmd, %region_2.4_spmd} | conditional | flops 275122944 | bytes 8596558 | solution.py:132
  191.6 1.7 fusion.6
  202.1 20.2 %all_to_all.15 = bf16[8,32,2048]{2,1,0:T(8,128)(2,1)S(1)} all-to-all(bf16[8,32,2048]{2,1,0:T(8,128)(2,1)S(1)} %bitcast.61), channel_id=1, replica_groups=mesh['sp'=64,'tp'=8] {'tp'}, dimensions={0} | all-to-all | bytes 2097152 | tf_op jit(solution)/shard_map/all_to_all | solution.py:41
  224.1 3.6 %all-to-all-start.1 = ((bf16[8,32,2048]{2,1,0:T(8,128)(2,1)}), bf16[8,32,2048]{2,1,0:T(8,128)(2,1)S(1)}, u32[]{:S(2)}, u32[]{:S(2)}) async-start(bf16[8,32,2048]{2,1,0:T(8,128)(2,1)} %broadcast_in_dim.49), calls=%async_computation.1 | async-start | bytes 2097152 | tf_op jit(solution)/shard_map/all_to_all | solution.py:53
  227.6 15.8 %all-to-all-done.1 = bf16[8,32,2048]{2,1,0:T(8,128)(2,1)S(1)} async-done(((bf16[8,32,2048]{2,1,0:T(8,128)(2,1)}), bf16[8,32,2048]{2,1,0:T(8,128)(2,1)S(1)}, u32[]{:S(2)}, u32[]{:S(2)}) %all-to-all-start.1) | async-done | bytes 1048608 | tf_op jit(solution)/shard_map/all_to_all | solution.py:53
  243.5 3.1 %fusion.24 = f32[256,512]{1,0:T(8,128)} fusion(bf16[256,2048]{1,0:T(8,128)(2,1)S(1)} %bitcast.62, bf16[2048,1536]{1,0:T(8,128)(2,1)} %all-gather.6.cloned.1.call-done), kind=kOutput, calls=%fused_computation.34 | convolution fusion | flops 536870912 | bytes 3670016 | tf_op jit(solution)/shard_map/dot_general | solution.py:173
  246.6 3.8 %convolution_convert_fusion = bf16[256,2048]{1,0:T(8,128)(2,1)S(1)} fusion(bf16[2048,1536]{1,0:T(8,128)(2,1)} %all-gather.6.cloned.1.call-done, bf16[256,2048]{1,0:T(8,128)(2,1)S(1)} %bitcast.63, f32[256,512]{1,0:T(8,128)} %fusion.24), kind=kOutput, calls=%fused_computation.29 | convolution fusion | flops 1075052544 | bytes 6815744 | tf_op jit(solution)/shard_map/dot_general | solution.py:178
  250.4 18.4 %all_to_all.16 = bf16[8,32,2048]{2,1,0:T(8,128)(2,1)S(1)} all-to-all(bf16[8,32,2048]{2,1,0:T(8,128)(2,1)S(1)} %bitcast.64), channel_id=1, replica_groups=mesh['sp'=64,'tp'=8] {'tp'}, dimensions={0} | all-to-all | bytes 2097152 | tf_op jit(solution)/shard_map/all_to_all | solution.py:41
  (206 shorter events, 72.9 us)
Async XLA Ops:
  6.5 195.1 %copy-start = (bf16[256,2048]{1,0:T(8,128)(2,1)S(1)}, bf16[256,2048]{1,0:T(8,128)(2,1)}, u32[]{:S(2)}) copy-start(bf16[256,2048]{1,0:T(8,128)(2,1)} %param.22) | copy-start | bytes 3145732
  6.5 100.9 %all-gather.4.cloned.1.call-start = ((), (), s32[]{:S(2)}) async-start(), calls=%async_computation.3 | async-start | bytes 8519680 | tf_op jit(solution)/shard_map/all_gather | solution.py:31
  8.2 219.4 %all-gather.6.cloned.1.call-start = ((), (), s32[]{:S(2)}) async-start(), calls=%async_computation.4 | async-start | bytes 6389760 | tf_op jit(solution)/shard_map/all_gather | solution.py:15
  59.0 54.2 %copy-start.3 = (s32[256]{0:T(256)S(1)}, s32[256]{0:T(256)}, u32[]{:S(2)}) copy-start(s32[256]{0:T(256)} %param.21) | copy-start | bytes 3076
  202.1 20.5 %copy-start.1 = (bf16[32,2048]{1,0:T(8,128)(2,1)S(1)}, bf16[32,2048]{1,0:T(8,128)(2,1)}, u32[]{:S(2)}) copy-start(bf16[32,2048]{1,0:T(8,128)(2,1)} %param.16) | copy-start | bytes 393220
  202.1 20.5 %copy-start.2 = (f32[2048]{0:T(1024)S(1)}, f32[2048]{0:T(1024)}, u32[]{:S(2)}) copy-start(f32[2048]{0:T(1024)} %param.23) | copy-start | bytes 24580
  202.1 20.7 %copy-start.4 = (f32[2048]{0:T(1024)S(1)}, f32[2048]{0:T(1024)}, u32[]{:S(2)}) copy-start(f32[2048]{0:T(1024)} %param.24) | copy-start | bytes 24580
  224.1 19.4 %all-to-all-start.1 = ((bf16[8,32,2048]{2,1,0:T(8,128)(2,1)}), bf16[8,32,2048]{2,1,0:T(8,128)(2,1)S(1)}, u32[]{:S(2)}, u32[]{:S(2)}) async-start(bf16[8,32,2048]{2,1,0:T(8,128)(2,1)} %broadcast_in_dim.49), calls=%async_computation.1 | async-start | bytes 2097152 | tf_op jit(solution)/shard_map/all_to_all | solution.py:53
Sparse Core Ops, SparseCore 0:
  10.4 97.0 all-gather.3
  110.5 87.1 all-gather.5
where the time goes:
time: 278 us; the launch traced here: 277 us
  blocking collectives  84.8 us (31%)
  waiting for transfers between devices  64.4 us (23%)
  matrix products  46 us (17%)
  local copies, waits for them, and re-layouts  28.4 us (10%)
  loops' own time  21.6 us (8%)
  other arithmetic  14.2 us (5%)
  between operations  13.6 us (5%)
  starting transfers between devices  3.6 us (1%)
    all_gather x1, waiting for transfers between devices, side_by_side(): lax.all_gather(both, axis, axis=dim, tiled=True)  48.5 us
    all_gather x1, blocking collectives, local(): lax.all_gather(documents, 'sp', axis=0, tiled=True)  46.2 us
    all_to_all x2, blocking collectives, sent_and_summed(): lax.all_to_all(blocks, axis, split_axis=0, concat_axis=0, tiled=True)  38.6 us
    another operation x1, loops' own time, local(): lax.fori_loop(0, key_count // block_len, advance, start_state)  20.9 us
    dot_general x12, matrix products, attend_block(): jnp.einsum('kgts,skd->kgtd', probs.astype(jnp.bfloat16), value_rows.resha...  19.9 us
    dot_general x12, matrix products, attend_block(): jnp.einsum('tkgd,skd->kgts', query_heads, key_rows.reshape(key_count, kv_...  18.8 us
    all_to_all x1, waiting for transfers between devices, sent_to_all(): lax.all_to_all(jnp.broadcast_to(array[None], (size, *array.shape)), axis,...  15.8 us
    slice x16, local copies, waits for them, and re-layouts, maybe_attend(): needed = (first_row <= own_last) & (doc_rows[-1] >= first_doc)  9.79 us
  transfers between devices with their start and end apart: 3, of which 2 were waited for; matrix products, arithmetic and copies ran while one was open for 29% of the time, Pallas kernels for 0%

commit v1 on v0

v1 whole, which is shorter than its diff:
```python
import functools
import math

import jax
import jax.numpy as jnp
from jax import lax
from jax.experimental import pallas as pl
from jax.experimental.pallas import tpu as pltpu
from jax.sharding import PartitionSpec as P

HD = 128
MESH = pl.DeviceIdType.MESH
HIDE = -1e30
FLOOR = -1e20
AUG = 16
F32 = jnp.float32
BF16 = jnp.bfloat16
Y_DIM = 8
A_LANES = 128


def dot(a, b):
    return jnp.dot(a, b, preferred_element_type=F32)


class Ring:
    def __init__(self, n, pos, core, device, items, send_sem, recv_sem):
        self.n, self.pos, self.core, self.device, self.items = n, pos, core, device, items
        self.send_sem, self.recv_sem = send_sem, recv_sem
        self.last = n // 2 - 1
        self.copies = {}

    def at(self, step):
        return lax.rem(self.pos + step + 2 * self.n, self.n)

    def send(self, s, subs=None):
        for sub in range(len(self.items)) if subs is None else subs:
            if s < self.last:
                ways = [(0, self.at(-s), self.at(1)), (1, self.at(s), self.at(-1))]
            else:
                way = 1 - 2 * self.core
                ways = [(0, self.at(-way * s), self.at(way))]
            for d, item, to in ways:
                ref = self.items[sub](item)
                copy = pltpu.make_async_remote_copy(
                    src_ref=ref,
                    dst_ref=ref,
                    send_sem=self.send_sem.at[d, s, sub],
                    recv_sem=self.recv_sem.at[d, s, sub],
                    device_id=self.device(to),
                    device_id_type=MESH,
                )
                copy.start()
                self.copies[d, s, sub] = copy

    def wait(self, s, subs=None):
        for sub in range(len(self.items)) if subs is None else subs:
            for d in range(2 if s < self.last else 1):
                self.copies[d, s, sub].wait_recv()

    def arrived(self, s):
        if s < self.last:
            return [self.at(-1 - s), self.at(1 + s)]
        return [self.at(self.n // 2)]

    def finish(self):
        for copy in self.copies.values():
            copy.wait_send()


def layer_kernel(
    nz,
    ny,
    nx,
    back,
    resid,
    q,
    k,
    v,
    gates,
    docs,
    outw,
    attn_gain,
    mlp_gain,
    wpack,
    out,
    qa,
    kf,
    vt,
    osend,
    orecv,
    ssend,
    srecv,
    acc,
    att,
    asib,
    wsib,
    ps1,
    pr1,
    nrm,
    ps2,
    pr2,
    mid,
    wall,
    hid,
    low,
    q_ss,
    q_rs,
    k_ss,
    k_rs,
    a1_ss,
    a1_rs,
    b1_ss,
    b1_rs,
    a2_ss,
    a2_rs,
    b2_ss,
    b2_rs,
    fwd_ss,
    fwd_rs,
    o_ss,
    o_rs,
    t_ss,
    t_rs,
    x_ss,
    x_rs,
    c_ss,
    c_rs,
):
    sp, tp = lax.axis_index("sp"), lax.axis_index("tp")
    z, y = lax.div(sp, ny), lax.rem(sp, ny)
    x, c = lax.div(tp, 2), lax.rem(tp, 2)
    rows = q.shape[0]
    own_rows, width = resid.shape
    hidden = wpack.shape[2]
    scale = 1.0 / math.sqrt(HD)
    scale2 = scale * math.log2(math.e)
    la = A_LANES

    def along_z(i):
        return (i * ny + y, tp)

    def along_y(i):
        return (z * ny + i, tp)

    def along_x(i):
        return (sp, 2 * i + c)

    sibling = (sp, 2 * x + 1 - c)

    barrier = pltpu.get_barrier_semaphore()
    greet = [along_z(lax.rem(z + d, nz)) for d in ([1, nz - 1] if nz > 2 else [1])]
    greet += [along_y(lax.rem(y + d, ny)) for d in range(1, ny)]
    greet += [along_x(lax.rem(x + d, nx)) for d in range(1, nx)]
    greet += [sibling]
    for device in greet:
        pl.semaphore_signal(barrier, inc=1, device_id=device, device_id_type=MESH)

    row16 = lax.broadcasted_iota(jnp.int32, (AUG, rows), 0)
    doc16 = jnp.broadcast_to(docs[...], (AUG, rows))
    for h in range(2):
        qa[y, 0:HD, h * rows : (h + 1) * rows] = (
            q[:, h * HD : (h + 1) * HD].astype(F32).T.astype(BF16)
        )
        one_hot = jnp.where((row16 < 3) & (doc16 == row16), 1.0, 0.0)
        pick = jnp.where((row16 >= 3 + 3 * h) & (row16 < 6 + 3 * h), 1.0, 0.0)
        qa[y, HD : HD + AUG, h * rows : (h + 1) * rows] = (one_hot + pick).astype(BF16)
    kf[z, :, 0:HD] = k[...]
    vt[z, 0:HD, :] = v[...].astype(F32).T.astype(BF16)
    vt[z, HD : HD + AUG, :] = jnp.where(row16 == 0, doc16.astype(F32), 0.0).astype(BF16)

    pl.semaphore_wait(barrier, len(greet))

    def remote(src, dst, ss, rs, device):
        copy = pltpu.make_async_remote_copy(
            src_ref=src,
            dst_ref=dst,
            send_sem=ss,
            recv_sem=rs,
            device_id=device,
            device_id_type=MESH,
        )
        copy.start()
        return copy

    k_ring = Ring(
        nz,
        z,
        c,
        along_z,
        [lambda i: kf.at[i, :, 0:HD], lambda i: vt.at[i]],
        k_ss,
        k_rs,
    )
    q_ring = Ring(
        ny,
        y,
        c,
        along_y,
        [
            lambda i: qa.at[i, 0 : HD + AUG, 0:rows],
            lambda i: qa.at[i, 0 : HD + AUG, rows : 2 * rows],
        ],
        q_ss,
        q_rs,
    )
    a1 = Ring(nz, z, c, along_z, [lambda i: wall.at[c, :, i, y, :, 0:la]], a1_ss, a1_rs)
    b1 = Ring(ny, y, c, along_y, [lambda i: wall.at[c, :, z, i, :, la:hidden]], b1_ss, b1_rs)
    a2 = Ring(
        ny,
        y,
        c,
        along_y,
        [lambda i, w=w: wall.at[c, w, :, i, :, 0:la] for w in range(3)],
        a2_ss,
        a2_rs,
    )
    b2 = Ring(
        nz,
        z,
        c,
        along_z,
        [lambda i, w=w: wall.at[c, w, i, :, :, la:hidden] for w in range(3)],
        b2_ss,
        b2_rs,
    )

    k_ring.send(0)
    q_ring.send(0)
    wall[c, :, z, y] = wpack[...]
    a1.send(0)
    b1.send(0)
    core_copies = [remote(outw, wsib, c_ss.at[0], c_rs.at[0], sibling)]

    def zero_rows(i, _):
        qa[i, HD + AUG :, :] = jnp.zeros((qa.shape[1] - HD - AUG, 2 * rows), BF16)
        return 0

    lax.fori_loop(0, ny, zero_rows, 0)

    def key_terms(i):
        first = pl.multiple_of(rows * (i * ny + y), rows)
        raised = gates[:, pl.ds(first, rows)] * (-1.0 / scale)
        high = raised.astype(BF16).astype(F32)
        middle = (raised - high).astype(BF16).astype(F32)
        lowest = raised - high - middle
        key_docs = vt[i, HD : HD + AUG, :].astype(F32)[0:1, :]
        terms = jnp.where(row16.astype(F32) == key_docs, 0.0, HIDE)
        terms = jnp.where(row16 < 3, terms, 0.0)
        for h in range(2):
            for j, piece in enumerate((high, middle, lowest)):
                terms = jnp.where(row16 == 3 + 3 * h + j, piece[h : h + 1, :], terms)
        tall = jnp.concatenate([terms, jnp.zeros((HD - AUG, rows), F32)], axis=0)
        kf[i, :, HD : 2 * HD] = tall.T.astype(BF16)

    key_terms(z)
    for s in range(1, max(nz, ny) // 2 + 1):
        for ring in (k_ring, q_ring, a1, b1):
            if s - 1 <= ring.last:
                ring.wait(s - 1)
            if s <= ring.last:
                ring.send(s)
        if s - 1 <= k_ring.last:
            for i in k_ring.arrived(s - 1):
                key_terms(i)

    forwards = []

    def forward_a(i):
        piece = wall.at[c, :, :, i, :, 0:la]
        at = len(forwards)
        forwards.append(remote(piece, piece, fwd_ss.at[at], fwd_rs.at[at], sibling))

    def forward_b(i):
        piece = wall.at[c, :, i, :, :, la:hidden]
        at = len(forwards)
        forwards.append(remote(piece, piece, fwd_ss.at[at], fwd_rs.at[at], sibling))

    b2.send(0)
    a2.send(0)
    forward_b(z)
    forward_a(y)

    pending_b = [(s, w) for s in range(b2.last + 1) for w in range(3)]
    pending_a = [(s, w) for s in range(a2.last + 1) for w in range(3)]

    def relay(ring, pending, forward, count):
        for _ in range(count):
            if not pending:
                return
            s, w = pending.pop(0)
            ring.wait(s, [w])
            if s < ring.last:
                ring.send(s + 1, [w])
            if w == 2:
                for i in ring.arrived(s):
                    forward(i)

    def attend(step, own):
        if own:
            yq = y
        else:
            odd = lax.rem(step, 2)
            half = lax.div(step + 1, 2)
            yq = lax.rem(y + ny // 2 + jnp.where(odd == 1, -half, half) + ny, ny)
        queries = qa[yq]
        raw = dot(kf[z], queries)
        key_at = lax.broadcasted_iota(jnp.int32, raw.shape, 0)
        col = lax.broadcasted_iota(jnp.int32, raw.shape, 1)
        query_at = jnp.where(col >= rows, col - rows, col)
        raw = jnp.where(query_at - key_at + rows * (yq - y) >= 0, raw, HIDE)
        top = jnp.maximum(jnp.max(raw, axis=0, keepdims=True) * scale2, FLOOR)
        probs = jnp.exp2(raw * scale2 - top)
        total = jnp.sum(probs, axis=0, keepdims=True)
        acc[...] = dot(vt[z, 0:HD, :], probs.astype(BF16))

        def more(i, state):
            top, total = state
            raw = dot(kf[i], queries)
            new = jnp.maximum(top, jnp.max(raw, axis=0, keepdims=True) * scale2)
            probs = jnp.exp2(raw * scale2 - new)
            shrink = jnp.exp2(top - new)
            total = total * shrink + jnp.sum(probs, axis=0, keepdims=True)
            acc[...] = acc[...] * shrink + dot(vt[i, 0:HD, :], probs.astype(BF16))
            return new, total

        top, total = lax.fori_loop(jnp.maximum(z - back, 0), z, more, (top, total))
        row8 = lax.broadcasted_iota(jnp.int32, (8, 2 * rows), 0)
        stats = jnp.where(row8 == 0, top, total)
        if own:
            orecv[y] = acc[...].astype(BF16)
            srecv[y] = stats
        else:
            osend[yq] = acc[...].astype(BF16)
            ssend[yq] = stats
            remote(osend.at[yq], orecv.at[y], o_ss.at[step], o_rs.at[step], along_y(yq))
            remote(ssend.at[yq], srecv.at[y], t_ss.at[step], t_rs.at[step], along_y(yq))

    def attend_steps(first, past):
        if past > first:
            lax.fori_loop(first, past, lambda s, _: (attend(s, False), 0)[1], 0)

    cuts = [0, min(3, ny - 1), min(5, ny - 1), ny - 1]
    attend_steps(cuts[0], cuts[1])
    relay(b2, pending_b, forward_b, 1)
    attend_steps(cuts[1], cuts[2])
    relay(b2, pending_b, forward_b, 1)
    relay(a2, pending_a, forward_a, 2)
    attend_steps(cuts[2], cuts[3])
    relay(b2, pending_b, forward_b, 1)
    relay(a2, pending_a, forward_a, 1)
    attend(ny - 1, True)
    relay(b2, pending_b, forward_b, 2)

    for step in range(ny - 1):
        pltpu.make_async_remote_copy(
            src_ref=osend.at[0],
            dst_ref=orecv.at[0],
            send_sem=o_ss.at[step],
            recv_sem=o_rs.at[step],
            device_id=sibling,
            device_id_type=MESH,
        ).wait()
        pltpu.make_async_remote_copy(
            src_ref=ssend.at[0],
            dst_ref=srecv.at[0],
            send_sem=t_ss.at[step],
            recv_sem=t_rs.at[step],
            device_id=sibling,
            device_id_type=MESH,
        ).wait()

    top = srecv[0, 0:1, :]
    for i in range(1, ny):
        top = jnp.maximum(top, srecv[i, 0:1, :])
    acc[...] = jnp.zeros(acc.shape, F32)

    def join(i, total):
        share = jnp.exp2(srecv[i, 0:1, :] - top)
        acc[...] += orecv[i].astype(F32) * share
        return total + share * srecv[i, 1:2, :]

    total = lax.fori_loop(0, ny, join, jnp.zeros(top.shape, F32))
    joined = acc[...] / total
    for h in range(2):
        part = joined[:, h * rows : (h + 1) * rows].T.astype(BF16)
        att[:, :, :, h * HD : (h + 1) * HD] = part.reshape(nx, 2, own_rows, HD)
    core_copies.append(remote(att.at[:, 1 - c], asib, c_ss.at[1], c_rs.at[1], sibling))
    relay(b2, pending_b, forward_b, 1)
    relay(a2, pending_a, forward_a, 3)
    for copy in core_copies:
        copy.wait()

    core_rows = nx * own_rows
    mine = att[:, c].reshape(core_rows, 2 * HD)
    theirs = asib[...].reshape(core_rows, 2 * HD)
    chunk = min(512, width)
    for at in range(0, width, chunk):
        part = dot(mine, outw[:, at : at + chunk]) + dot(theirs, wsib[:, at : at + chunk])
        ps1[:, :, at : at + chunk] = part.astype(BF16).reshape(nx, own_rows, chunk)

    def to_owners(send, recv, which):
        copies = []
        for d in range(1, nx):
            to = lax.rem(x + d, nx)
            sems = (x_ss.at[which, d - 1], x_rs.at[which, d - 1])
            copies.append(remote(send.at[to], recv.at[x], *sems, along_x(to)))
        return copies

    def summed(send, recv):
        sums = send[x].astype(F32)
        for d in range(1, nx):
            sums = sums + recv[lax.rem(x + d, nx)].astype(F32)
        return sums

    copies = to_owners(ps1, pr1, 0)
    relay(b2, pending_b, forward_b, 1)
    relay(a2, pending_a, forward_a, 1)
    for copy in copies:
        copy.wait()
    projected = summed(ps1, pr1)
    power = jnp.mean(projected * projected, axis=-1, keepdims=True)
    middle = resid[...].astype(F32) + attn_gain[...] * projected * lax.rsqrt(power + 1e-06)
    mid[...] = middle
    middle_power = jnp.mean(middle * middle, axis=-1, keepdims=True)
    nrm[x] = (mlp_gain[...] * middle * lax.rsqrt(middle_power + 1e-06)).astype(BF16)
    copies = []
    for d in range(1, nx):
        sems = (x_ss.at[1, d - 1], x_rs.at[1, d - 1])
        copies.append(remote(nrm.at[x], nrm.at[x], *sems, along_x(lax.rem(x + d, nx))))
    relay(b2, pending_b, forward_b, 2)
    relay(a2, pending_a, forward_a, 2)
    for copy in copies:
        copy.wait()
    relay(b2, pending_b, forward_b, len(pending_b))
    relay(a2, pending_a, forward_a, len(pending_a))
    for copy in forwards:
        copy.wait()

    normed = nrm[...].reshape(core_rows, width)
    low[...] = jnp.zeros(low.shape, F32)

    def feed(j, _):
        gate = dot(normed, wall[j, 0].reshape(width, hidden))
        up = dot(normed, wall[j, 1].reshape(width, hidden))
        hid[...] = (gate / (1.0 + jnp.exp(-gate)) * up).astype(BF16)
        zs = max(1, chunk * nz // width)
        for at in range(0, nz, zs):
            w = wall[j, 2, at : at + zs].reshape(zs * width // nz, hidden)
            cols = slice(at * width // nz, (at + zs) * width // nz)
            low[:, cols] += lax.dot_general(
                hid[...], w, (((1,), (1,)), ((), ())), preferred_element_type=F32
            )
        return 0

    lax.fori_loop(0, 2, feed, 0)
    ps2[...] = low[...].astype(BF16).reshape(nx, own_rows, width)
    for copy in to_owners(ps2, pr2, 2):
        copy.wait()
    out[...] = (mid[...] + 0.5 * summed(ps2, pr2)).astype(BF16)
    for ring in (k_ring, q_ring, a1, b1, a2, b2):
        ring.finish()


def make_local(nz, ny, nx, back):
    def local(
        resid,
        queries,
        keys,
        values,
        log_gates,
        documents,
        out_weight,
        attn_gain,
        mlp_gain,
        gate_weight,
        up_weight,
        down_weight,
    ):
        rows = queries.shape[0]
        own_rows, width = resid.shape
        w_rows, hidden = gate_weight.shape
        wpack = jnp.stack([gate_weight, up_weight, down_weight.T])
        dma = pltpu.SemaphoreType.DMA
        x_block = pltpu.VMEM((nx, own_rows, width), BF16)
        kz, ky = nz // 2, ny // 2
        scratch = [
            pltpu.VMEM((ny, 2 * HD, 2 * rows), BF16),
            pltpu.VMEM((nz, rows, 2 * HD), BF16),
            pltpu.VMEM((nz, HD + AUG, rows), BF16),
            pltpu.VMEM((ny, HD, 2 * rows), BF16),
            pltpu.VMEM((ny, HD, 2 * rows), BF16),
            pltpu.VMEM((ny, 8, 2 * rows), F32),
            pltpu.VMEM((ny, 8, 2 * rows), F32),
            pltpu.VMEM((HD, 2 * rows), F32),
            pltpu.VMEM((nx, 2, own_rows, 2 * HD), BF16),
            pltpu.VMEM((nx, own_rows, 2 * HD), BF16),
            pltpu.VMEM(out_weight.shape, BF16),
            x_block,
            x_block,
            x_block,
            x_block,
            x_block,
            pltpu.VMEM((own_rows, width), F32),
            pltpu.VMEM((2, 3, nz, ny, w_rows, hidden), BF16),
            pltpu.VMEM((nx * own_rows, hidden), BF16),
            pltpu.VMEM((nx * own_rows, width), F32),
        ]
        for steps, subs in ((ky, 2), (kz, 2), (kz, 1), (ky, 1), (ky, 3), (kz, 3)):
            scratch += [dma((2, steps, subs)), dma((2, steps, subs))]
        scratch += [dma((nz + ny,)), dma((nz + ny,))]
        scratch += [dma((ny - 1,))] * 4
        scratch += [dma((3, max(nx - 1, 1)))] * 2
        scratch += [dma((2,)), dma((2,))]
        vmem = pl.BlockSpec(memory_space=pltpu.VMEM)
        return pl.pallas_call(
            functools.partial(layer_kernel, nz, ny, nx, back),
            out_shape=jax.ShapeDtypeStruct((own_rows, width), BF16),
            in_specs=[vmem] * 10,
            out_specs=vmem,
            scratch_shapes=scratch,
            compiler_params=pltpu.CompilerParams(
                collective_id=0, has_side_effects=True, vmem_limit_bytes=60 * 1024 * 1024
            ),
        )(
            resid,
            queries,
            keys,
            values,
            log_gates,
            documents.reshape(1, rows),
            out_weight,
            attn_gain.reshape(1, width),
            mlp_gain.reshape(1, width),
            wpack,
        )

    return local


def solution(mesh, ny=Y_DIM):
    blocks, tp = mesh.shape["sp"], mesh.shape["tp"]
    nz, nx = blocks // ny, tp // 2
    back = min((3 * blocks // 4 + ny - 1) // ny, nz - 1)
    placed = (
        P(("sp", "tp"), None),
        P("sp", "tp"),
        P("sp", "tp"),
        P("sp", "tp"),
        P("tp", None),
        P("sp"),
        P("tp", None),
        P(),
        P(),
        P("sp", "tp"),
        P("sp", "tp"),
        P("tp", "sp"),
    )
    return jax.shard_map(
        make_local(nz, ny, nx, back),
        mesh=mesh,
        in_specs=placed,
        out_specs=P(("sp", "tp"), None),
        check_vma=False,
    )
```

time: 278 us -> 111 us (0.40)
  the two profiles are of different devices: /device:TPU:368 before, /device:TPU:8 now
where the time goes in v1:
time: 111 us; the launch traced here: 110 us
  Pallas kernels  107 us (96%)
  local copies, waits for them, and re-layouts  1.57 us (1%)
  other arithmetic  1.44 us (1%)
    pallas_call x1, Pallas kernels, local(): pl.pallas_call(functools.partial(layer_kernel, nz, ny, nx, back), out_sha...  107 us

profile of v1, /device:TPU:8, one launch (start us, length us, event | category | flops | bytes accessed | tf_op | source)
XLA Modules:
  0.0 110.4 jit_solution(4652800687437509795)
XLA Ops:
  0.0 1.4 %pad_maximum_fusion.wpack = bf16[3,32,512]{2,1,0:T(8,128)(2,1)} fusion(bf16[1,32,512]{2,1,0:T(8,128)(2,1)} %bitcast.8, bf16[1,32,512]{2,1,0:T(8,128)(2,1)} %bitcast.9, bf16[1,32,512]{2,1,0:T(8,128)(2,1)} %bitcast.10), kind=kLoop, calls=%fused_computation | loop fusion | flops 98304 | bytes 196608 | tf_op jit(solution)/shard_map/stack | solution.py:483
  1.4 107.4 %shard_map.118 = bf16[32,2048]{1,0:T(8,128)(2,1)} custom-call(bf16[32,2048]{1,0:T(8,128)(2,1)} %resid.1, bf16[256,256]{1,0:T(8,128)(2,1)} %q.1, bf16[256,128]{1,0:T(8,128)(2,1)} %k.1, bf16[256,128]{1,0:T(8,128)(2,1)} %v.1, f32[2,16384]{1,0:T(2,128)} %gates.1, s32[1,256]{1,0:T(1,128)} %bitcast.13, bf16[256,2048]{1,0:T(8,128)(2,1)} %outw.1, ...), custom_call_target="tpu_custom_call" | custom-call | tf_op jit(solution)/shard_map/pallas_call | solution.py:516
  108.9 1.6 %copy.14 = bf16[32,2048]{1,0:T(8,128)(2,1)} copy(bf16[32,2048]{1,0:T(8,128)(2,1)} %shard_map.118) | data formatting | bytes 262144

commit v2 on v1

v2 whole, which is shorter than its diff:
```python
import contextlib
import functools
import math

import jax
import jax.numpy as jnp
from jax import lax
from jax.experimental import pallas as pl
from jax.experimental.pallas import tpu as pltpu
from jax.sharding import PartitionSpec as P

HD = 128
MESH = pl.DeviceIdType.MESH
HIDE = -1e30
FLOOR = -1e20
AUG = 16
F32 = jnp.float32
BF16 = jnp.bfloat16
Y_DIM = 8
A_LANES = (128, 256, 256)
PROFILE = False


def phase(name):
    return jax.named_scope(name) if PROFILE else contextlib.nullcontext()


def dot(a, b):
    return jnp.dot(a, b, preferred_element_type=F32)


class Ring:
    def __init__(self, n, pos, core, device, items, send_sem, recv_sem):
        self.n, self.pos, self.core, self.device, self.items = n, pos, core, device, items
        self.send_sem, self.recv_sem = send_sem, recv_sem
        self.last = n // 2 - 1
        self.copies = {}

    def at(self, step):
        return lax.rem(self.pos + step + 2 * self.n, self.n)

    def send(self, s, subs=None):
        for sub in range(len(self.items)) if subs is None else subs:
            if s < self.last:
                ways = [(0, self.at(-s), self.at(1)), (1, self.at(s), self.at(-1))]
            else:
                way = 1 - 2 * self.core
                ways = [(0, self.at(-way * s), self.at(way))]
            for d, item, to in ways:
                ref = self.items[sub](item)
                copy = pltpu.make_async_remote_copy(
                    src_ref=ref,
                    dst_ref=ref,
                    send_sem=self.send_sem.at[d, s, sub],
                    recv_sem=self.recv_sem.at[d, s, sub],
                    device_id=self.device(to),
                    device_id_type=MESH,
                )
                copy.start()
                self.copies[d, s, sub] = copy

    def wait(self, s, subs=None):
        for sub in range(len(self.items)) if subs is None else subs:
            for d in range(2 if s < self.last else 1):
                self.copies[d, s, sub].wait_recv()

    def arrived(self, s):
        if s < self.last:
            return [self.at(-1 - s), self.at(1 + s)]
        return [self.at(self.n // 2)]

    def finish(self):
        for copy in self.copies.values():
            copy.wait_send()


def layer_kernel(
    nz,
    ny,
    nx,
    back,
    resid,
    q,
    k,
    v,
    gates,
    docs,
    outw,
    attn_gain,
    mlp_gain,
    wpack,
    out,
    qa,
    kf,
    vt,
    osend,
    oin,
    ssend,
    sin,
    stats,
    raw,
    acc,
    att,
    attall,
    wo,
    rall,
    nrm,
    ps2,
    pr2,
    mid,
    wall,
    gact,
    hid,
    low,
    q_ss,
    q_rs,
    k_ss,
    k_rs,
    a1_ss,
    a1_rs,
    b1_ss,
    b1_rs,
    a2_ss,
    a2_rs,
    b2_ss,
    b2_rs,
    fwd_ss,
    fwd_rs,
    o_ss,
    o_rs,
    t_ss,
    t_rs,
    x_ss,
    x_rs,
    w_ss,
    w_rs,
    wf_ss,
    wf_rs,
    g_ss,
    g_rs,
    l_ss,
):
    sp, tp = lax.axis_index("sp"), lax.axis_index("tp")
    z, y = lax.div(sp, ny), lax.rem(sp, ny)
    x, c = lax.div(tp, 2), lax.rem(tp, 2)
    rows = q.shape[0]
    own_rows, width = resid.shape
    hidden = wpack.shape[2]
    scale = 1.0 / math.sqrt(HD)
    scale2 = scale * math.log2(math.e)
    la = [min(lanes, hidden - 128) for lanes in A_LANES]

    def along_z(i):
        return (i * ny + y, tp)

    def along_y(i):
        return (z * ny + i, tp)

    def along_x(i):
        return (sp, 2 * i + c)

    sibling = (sp, 2 * x + 1 - c)

    barrier = pltpu.get_barrier_semaphore()
    greet = [along_z(lax.rem(z + d, nz)) for d in ([1, nz - 1] if nz > 2 else [1])]
    greet += [along_y(lax.rem(y + d, ny)) for d in range(1, ny)]
    greet += [along_x(lax.rem(x + d, nx)) for d in range(1, nx)]
    greet += [sibling]
    for device in greet:
        pl.semaphore_signal(barrier, inc=1, device_id=device, device_id_type=MESH)

    own_wo = pltpu.make_async_copy(outw, wo.at[tp], l_ss)
    own_wo.start()

    with phase("prep"):
        row16 = lax.broadcasted_iota(jnp.int32, (AUG, rows), 0)
        doc16 = jnp.broadcast_to(docs[...], (AUG, rows))
        for h in range(2):
            qa[y, 0:HD, h * rows : (h + 1) * rows] = (
                q[:, h * HD : (h + 1) * HD].astype(F32).T.astype(BF16)
            )
            one_hot = jnp.where((row16 < 3) & (doc16 == row16), 1.0, 0.0)
            pick = jnp.where((row16 >= 3 + 3 * h) & (row16 < 6 + 3 * h), 1.0, 0.0)
            qa[y, HD : HD + AUG, h * rows : (h + 1) * rows] = (one_hot + pick).astype(BF16)
        kf[z, :, 0:HD] = k[...]
        vt[z, 0:HD, :] = v[...].astype(F32).T.astype(BF16)
        vt[z, HD : HD + AUG, :] = jnp.where(row16 == 0, doc16.astype(F32), 0.0).astype(BF16)

    with phase("barrier_wait"):
        pl.semaphore_wait(barrier, len(greet))

    def remote(src, dst, ss, rs, device):
        copy = pltpu.make_async_remote_copy(
            src_ref=src,
            dst_ref=dst,
            send_sem=ss,
            recv_sem=rs,
            device_id=device,
            device_id_type=MESH,
        )
        copy.start()
        return copy

    k_ring = Ring(
        nz,
        z,
        c,
        along_z,
        [lambda i: kf.at[i, :, 0:HD], lambda i: vt.at[i]],
        k_ss,
        k_rs,
    )
    q_ring = Ring(
        ny,
        y,
        c,
        along_y,
        [
            lambda i: qa.at[i, 0 : HD + AUG, 0:rows],
            lambda i: qa.at[i, 0 : HD + AUG, rows : 2 * rows],
        ],
        q_ss,
        q_rs,
    )
    a1 = Ring(
        nz,
        z,
        c,
        along_z,
        [lambda i, w=w: wall.at[c, w, i, y, :, 0 : la[w]] for w in range(3)],
        a1_ss,
        a1_rs,
    )
    b1 = Ring(
        ny,
        y,
        c,
        along_y,
        [lambda i, w=w: wall.at[c, w, z, i, :, la[w] : hidden] for w in range(3)],
        b1_ss,
        b1_rs,
    )
    a2 = Ring(
        ny,
        y,
        c,
        along_y,
        [lambda i, w=w: wall.at[c, w, :, i, :, 0 : la[w]] for w in range(3)],
        a2_ss,
        a2_rs,
    )
    b2 = Ring(
        nz,
        z,
        c,
        along_z,
        [lambda i, w=w: wall.at[c, w, i, :, :, la[w] : hidden] for w in range(3)],
        b2_ss,
        b2_rs,
    )
    heads_half = outw.shape[0] // 2
    wo_ring = Ring(
        nx,
        x,
        c,
        along_x,
        [lambda i, u=u: wo.at[2 * i + c, u * heads_half : (u + 1) * heads_half] for u in range(2)],
        w_ss,
        w_rs,
    )

    wall[c, :, z, y] = wpack[...]
    k_ring.send(0, [0])
    q_ring.send(0, [0])
    a1.send(0)
    b1.send(0)
    k_ring.send(0, [1])
    q_ring.send(0, [1])

    wo_forwards = []

    def forward_wo(i, u):
        piece = wo.at[2 * i + c, u * heads_half : (u + 1) * heads_half]
        at = len(wo_forwards)
        wo_forwards.append(remote(piece, piece, wf_ss.at[at], wf_rs.at[at], sibling))

    own_wo.wait()
    if nx > 1:
        wo_ring.send(0)
    for u in range(2):
        forward_wo(x, u)
    pending_wo = [(s, u) for s in range(nx // 2) for u in range(2)]

    def relay_wo(count):
        for _ in range(min(count, len(pending_wo))):
            s, u = pending_wo.pop(0)
            with phase("wo_wait"):
                wo_ring.wait(s, [u])
            if s < wo_ring.last:
                wo_ring.send(s + 1, [u])
            for i in wo_ring.arrived(s):
                forward_wo(i, u)

    def zero_rows(i, _):
        qa[i, HD + AUG :, :] = jnp.zeros((qa.shape[1] - HD - AUG, 2 * rows), BF16)
        return 0

    lax.fori_loop(0, ny, zero_rows, 0)

    def key_terms(i):
        first = pl.multiple_of(rows * (i * ny + y), rows)
        raised = gates[:, pl.ds(first, rows)] * (-1.0 / scale)
        high = raised.astype(BF16).astype(F32)
        middle = (raised - high).astype(BF16).astype(F32)
        lowest = raised - high - middle
        key_docs = vt[i, HD : HD + AUG, :].astype(F32)[0:1, :]
        terms = jnp.where(row16.astype(F32) == key_docs, 0.0, HIDE)
        terms = jnp.where(row16 < 3, terms, 0.0)
        for h in range(2):
            for j, piece in enumerate((high, middle, lowest)):
                terms = jnp.where(row16 == 3 + 3 * h + j, piece[h : h + 1, :], terms)
        tall = jnp.concatenate([terms, jnp.zeros((HD - AUG, rows), F32)], axis=0)
        kf[i, :, HD : 2 * HD] = tall.T.astype(BF16)

    forwards = [[], [], []]

    def forward(piece, w):
        at = len(forwards[w])
        forwards[w].append(remote(piece, piece, fwd_ss.at[w, at], fwd_rs.at[w, at], sibling))

    def forward_a(i, w):
        forward(wall.at[c, w, :, i, :, 0 : la[w]], w)

    def forward_b(i, w):
        forward(wall.at[c, w, i, :, :, la[w] : hidden], w)

    def step_on(ring, s, subs):
        if s <= ring.last:
            for sub in subs:
                with phase("ring_wait"):
                    ring.wait(s, [sub])
                if s < ring.last:
                    ring.send(s + 1, [sub])

    key_terms(z)
    for s in range(max(nz, ny) // 2):
        step_on(k_ring, s, [0])
        step_on(q_ring, s, [0])
        step_on(a1, s, [0, 1, 2])
        step_on(b1, s, [0, 1, 2])
        if s == b1.last:
            b2.send(0)
        if s == a1.last:
            a2.send(0)
        step_on(k_ring, s, [1])
        step_on(q_ring, s, [1])
        if s <= k_ring.last:
            for i in k_ring.arrived(s):
                key_terms(i)
    for w in range(3):
        forward_b(z, w)
        forward_a(y, w)

    pending_b = [(s, w) for s in range(b2.last + 1) for w in range(3)]
    pending_a = [(s, w) for s in range(a2.last + 1) for w in range(3)]

    def relay(ring, pending, onward, count):
        for _ in range(min(count, len(pending))):
            s, w = pending.pop(0)
            with phase("relay_wait"):
                ring.wait(s, [w])
            if s < ring.last:
                ring.send(s + 1, [w])
            for i in ring.arrived(s):
                onward(i, w)

    def relay_a(count):
        relay(a2, pending_a, forward_a, count)

    def relay_b(count):
        relay(b2, pending_b, forward_b, count)

    half = ny // 2
    first_block = jnp.maximum(z - back, 0)
    count = z - first_block

    def query_block(step):
        odd = lax.rem(step, 2)
        turn = lax.div(step + 1, 2)
        return lax.rem(y + half + jnp.where(odd == 1, -turn, turn) + ny, ny)

    def fold(a, op):
        return op(a.reshape(rows // 8, 8, 2 * rows), axis=0)

    def score(slot, j, i, yq, diagonal):
        found = dot(kf[i], qa[yq])
        if diagonal:
            key_at = lax.broadcasted_iota(jnp.int32, found.shape, 0)
            col = lax.broadcasted_iota(jnp.int32, found.shape, 1)
            query_at = jnp.where(col >= rows, col - rows, col)
            found = jnp.where(query_at - key_at + rows * (yq - y) >= 0, found, HIDE)
        raw[slot, j] = found
        return fold(found, jnp.max)

    def weigh(slot, j, top):
        probs = jnp.exp2(raw[slot, j] * scale2 - top)
        return fold(probs, jnp.sum), probs.astype(BF16)

    def highest(top8):
        return jnp.maximum(jnp.max(top8, axis=0, keepdims=True) * scale2, FLOOR)

    def first_scores():
        yq = query_block(0)
        top8 = score(0, 0, z, yq, True)

        def more(j, top8):
            return jnp.maximum(top8, score(0, j, first_block + j - 1, yq, False))

        return lax.fori_loop(1, count + 1, more, top8)

    def attend(step, top8):
        slot = lax.rem(step, 2)
        top = highest(top8)
        ahead = query_block(step + 1)
        next8 = score(1 - slot, 0, z, ahead, True)
        sum8, probs = weigh(slot, 0, top)
        acc[...] = dot(vt[z, 0:HD, :], probs)

        def more(j, state):
            next8, sum8 = state
            i = first_block + j - 1
            next8 = jnp.maximum(next8, score(1 - slot, j, i, ahead, False))
            part8, probs = weigh(slot, j, top)
            acc[...] += dot(vt[i, 0:HD, :], probs)
            return next8, sum8 + part8

        next8, sum8 = lax.fori_loop(1, count + 1, more, (next8, sum8))
        row8 = lax.broadcasted_iota(jnp.int32, (8, 2 * rows), 0)
        stats[...] = jnp.where(row8 == 0, top, jnp.sum(sum8, axis=0, keepdims=True))
        return next8

    def lanes(h):
        return slice(h * rows, (h + 1) * rows)

    def out_copy(step, d, j, h, to):
        return pltpu.make_async_remote_copy(
            src_ref=osend.at[step, :, lanes(h)],
            dst_ref=oin.at[d, j, :, lanes(h)],
            send_sem=o_ss.at[step, h],
            recv_sem=o_rs.at[d, j, h],
            device_id=to,
            device_id_type=MESH,
        )

    def stat_copy(step, d, j, to):
        return pltpu.make_async_remote_copy(
            src_ref=ssend.at[step],
            dst_ref=sin.at[d, j],
            send_sem=t_ss.at[step],
            recv_sem=t_rs.at[d, j],
            device_id=to,
            device_id_type=MESH,
        )

    def add_arrived(d, j, after):
        with phase("o_wait"):
            stat_copy(0, d, j, sibling).wait_recv()
        top = stats[0:1, :]
        other = sin[d, j, 0:1, :]
        new = jnp.maximum(top, other)
        keep = jnp.exp2(top - new)
        take = jnp.exp2(other - new)
        total = stats[1:2, :] * keep + sin[d, j, 1:2, :] * take
        row8 = lax.broadcasted_iota(jnp.int32, (8, 2 * rows), 0)
        stats[...] = jnp.where(row8 == 0, new, total)
        for h in range(2):
            at = lanes(h)
            with phase("o_wait"):
                out_copy(0, d, j, h, sibling).wait_recv()
            acc[:, at] = acc[:, at] * keep[:, at] + oin[d, j, :, at].astype(F32) * take[:, at]
            after(h)

    def pass_on(step):
        j = half - (step + 1) // 2
        d = c if step == 0 else 1 - step % 2
        to = along_y(lax.rem(y + 1 - 2 * d + ny, ny))

        def send(h):
            if h == 0:
                ssend[step] = stats[...]
                stat_copy(step, d, j - 1, to).start()
            osend[step, :, lanes(h)] = acc[:, lanes(h)].astype(BF16)
            out_copy(step, d, j - 1, h, to).start()

        def plain():
            send(0)
            send(1)

        if step == 0:
            plain()
        elif j < half - 1:
            add_arrived(d, j, send)
        else:
            pl.when(c == d)(lambda: add_arrived(d, j, send))
            pl.when(c != d)(plain)

    with phase("first_scores"):
        top8 = first_scores()
    plan = {
        0: (0, 0, 1),
        1: (1, 1, 0),
        2: (1, 1, 0),
        3: (1, 1, 1),
        4: (0, 1, 0),
        5: (1, 1, 1),
        6: (1, 0, 0),
        7: (1, 1, 1),
    }
    for step in range(ny):
        with phase("attend"):
            top8 = attend(step, top8)
        if step < ny - 1:
            pass_on(step)
        count_b, count_a, count_wo = plan[step]
        relay_b(count_b)
        relay_a(count_a)
        relay_wo(count_wo)
    relay_wo(len(pending_wo))
    rall[x] = resid[...]
    copies_r = []
    for d in range(1, nx):
        sems = (x_ss.at[1, d - 1], x_rs.at[1, d - 1])
        copies_r.append(remote(rall.at[x], rall.at[x], *sems, along_x(lax.rem(x + d, nx))))
    for d in range(2):
        if half > 1:
            add_arrived(d, 0, lambda h: None)
        else:
            pl.when(c == d)(functools.partial(add_arrived, d, 0, lambda h: None))
    with phase("join"):
        joined = acc[...] / stats[1:2, :]
        for h in range(2):
            part = joined[:, lanes(h)].T.astype(BF16).reshape(nx, 2, own_rows, HD)
            for core in range(2):
                att[core, :, :, h * HD : (h + 1) * HD] = part[:, core]

    got = []
    for dx in range(nx):
        for dc in range(2):
            if dx + dc:
                to = (sp, 2 * lax.rem(x + dx, nx) + jnp.where(dc == 1, 1 - c, c))
                at = 2 * dx + dc - 1
                core = to[1] - 2 * lax.div(to[1], 2)
                copy = remote(att.at[core], attall.at[tp], g_ss.at[at], g_rs.at[at], to)
                source = 2 * lax.rem(x - dx + nx, nx) + jnp.where(dc == 1, 1 - c, c)
                got.append((copy, source, dx))
    core_rows = nx * own_rows
    chunk = min(512, width)
    relay_a(1)

    def project(first, block, source):
        for at in range(0, width, chunk):
            part = dot(block, wo[source, :, at : at + chunk])
            if first:
                low[:, at : at + chunk] = part
            else:
                low[:, at : at + chunk] += part

    with phase("outproj"):
        project(True, att[c].reshape(core_rows, 2 * HD), tp)
    with phase("fwo_wait"):
        for copy in wo_forwards:
            copy.wait()
    got.sort(key=lambda g: min(g[2], nx - g[2]))
    for n, (copy, source, _) in enumerate(got):
        with phase("ag_wait"):
            copy.wait()
        with phase("outproj"):
            project(False, attall[source].reshape(core_rows, 2 * HD), source)
        if n in (2, 4, 6):
            relay_b(1)
            relay_a(1 if n > 2 else 0)
    for copy in copies_r:
        copy.wait()

    def normalize(i, _):
        span = pl.ds(pl.multiple_of(i * own_rows, own_rows), own_rows)
        projected = low[span, :]
        power = jnp.mean(projected * projected, axis=-1, keepdims=True)
        middle = rall[i].astype(F32) + attn_gain[...] * projected * lax.rsqrt(power + 1e-06)
        mid[i] = middle
        middle_power = jnp.mean(middle * middle, axis=-1, keepdims=True)
        nrm[i] = (mlp_gain[...] * middle * lax.rsqrt(middle_power + 1e-06)).astype(BF16)
        return 0

    with phase("norm"):
        lax.fori_loop(0, nx, normalize, 0)
    while pending_b or pending_a:
        relay_b(1)
        relay_a(1)

    def forwarded(w):
        with phase("fwd_wait"):
            for copy in forwards[w]:
                copy.wait()

    normed = nrm[...].reshape(core_rows, width)

    def gate_core(j, _):
        gact[j] = dot(normed, wall[j, 0].reshape(width, hidden))
        return 0

    def up_core(j, _):
        gate = gact[j]
        up = dot(normed, wall[j, 1].reshape(width, hidden))
        hid[j] = (gate / (1.0 + jnp.exp(-gate)) * up).astype(BF16)
        return 0

    zs = max(1, chunk * nz // width)

    def down_cols(n, _):
        sums = 0.0
        for j in range(2):
            w = wall[j, 2, pl.ds(n * zs, zs)].reshape(zs * width // nz, hidden)
            sums += lax.dot_general(
                hid[j], w, (((1,), (1,)), ((), ())), preferred_element_type=F32
            )
        size = zs * width // nz
        cols = pl.ds(pl.multiple_of(n * size, size), size)
        ps2[:, :, cols] = sums.astype(BF16).reshape(nx, own_rows, size)
        return 0

    forwarded(0)
    with phase("ffn_gate"):
        lax.fori_loop(0, 2, gate_core, 0)
    forwarded(1)
    with phase("ffn_up"):
        lax.fori_loop(0, 2, up_core, 0)
    forwarded(2)
    with phase("ffn_down"):
        lax.fori_loop(0, nz // zs, down_cols, 0)

    def to_owners(send, recv, which):
        copies = []
        for d in range(1, nx):
            to = lax.rem(x + d, nx)
            sems = (x_ss.at[which, d - 1], x_rs.at[which, d - 1])
            copies.append(remote(send.at[to], recv.at[x], *sems, along_x(to)))
        return copies

    def summed(send, recv):
        sums = send[x].astype(F32)
        for d in range(1, nx):
            sums = sums + recv[lax.rem(x + d, nx)].astype(F32)
        return sums

    with phase("rs2_wait"):
        for copy in to_owners(ps2, pr2, 0):
            copy.wait()
    out[...] = (mid[x] + 0.5 * summed(ps2, pr2)).astype(BF16)
    for ring in (k_ring, q_ring, a1, b1, a2, b2, wo_ring):
        ring.finish()
    for step in range(ny - 1):
        stat_copy(step, 0, 0, sibling).wait_send()
        for h in range(2):
            out_copy(step, 0, 0, h, sibling).wait_send()


def make_local(nz, ny, nx, back):
    def local(
        resid,
        queries,
        keys,
        values,
        log_gates,
        documents,
        out_weight,
        attn_gain,
        mlp_gain,
        gate_weight,
        up_weight,
        down_weight,
    ):
        rows = queries.shape[0]
        own_rows, width = resid.shape
        w_rows, hidden = gate_weight.shape
        wpack = jnp.stack([gate_weight, up_weight, down_weight.T])
        dma = pltpu.SemaphoreType.DMA
        x_block = pltpu.VMEM((nx, own_rows, width), BF16)
        kz, ky = nz // 2, ny // 2
        scratch = [
            pltpu.VMEM((ny, 2 * HD, 2 * rows), BF16),
            pltpu.VMEM((nz, rows, 2 * HD), BF16),
            pltpu.VMEM((nz, HD + AUG, rows), BF16),
            pltpu.VMEM((ny - 1, HD, 2 * rows), BF16),
            pltpu.VMEM((2, ky, HD, 2 * rows), BF16),
            pltpu.VMEM((ny - 1, 8, 2 * rows), F32),
            pltpu.VMEM((2, ky, 8, 2 * rows), F32),
            pltpu.VMEM((8, 2 * rows), F32),
            pltpu.VMEM((2, back + 1, rows, 2 * rows), F32),
            pltpu.VMEM((HD, 2 * rows), F32),
            pltpu.VMEM((2, nx, own_rows, 2 * HD), BF16),
            pltpu.VMEM((2 * nx, nx, own_rows, 2 * HD), BF16),
            pltpu.VMEM((2 * nx, *out_weight.shape), BF16),
            x_block,
            x_block,
            x_block,
            x_block,
            pltpu.VMEM((nx, own_rows, width), F32),
            pltpu.VMEM((2, 3, nz, ny, w_rows, hidden), BF16),
            pltpu.VMEM((2, nx * own_rows, hidden), F32),
            pltpu.VMEM((2, nx * own_rows, hidden), BF16),
            pltpu.VMEM((nx * own_rows, width), F32),
        ]
        for steps, subs in ((ky, 2), (kz, 2), (kz, 3), (ky, 3), (ky, 3), (kz, 3)):
            scratch += [dma((2, steps, subs)), dma((2, steps, subs))]
        scratch += [dma((3, nz + ny)), dma((3, nz + ny))]
        scratch += [dma((ny - 1, 2)), dma((2, ky, 2)), dma((ny - 1,)), dma((2, ky))]
        scratch += [dma((2, max(nx - 1, 1)))] * 2
        scratch += [dma((2, max(nx // 2, 1), 2))] * 2
        scratch += [dma((2 * nx,))] * 2
        scratch += [dma((2 * nx,))] * 2
        scratch += [dma]
        vmem = pl.BlockSpec(memory_space=pltpu.VMEM)
        return pl.pallas_call(
            functools.partial(layer_kernel, nz, ny, nx, back),
            out_shape=jax.ShapeDtypeStruct((own_rows, width), BF16),
            in_specs=[vmem] * 6 + [pl.BlockSpec(memory_space=pl.ANY)] + [vmem] * 3,
            out_specs=vmem,
            scratch_shapes=scratch,
            compiler_params=pltpu.CompilerParams(
                collective_id=0, has_side_effects=True, vmem_limit_bytes=60 * 1024 * 1024
            ),
        )(
            resid,
            queries,
            keys,
            values,
            log_gates,
            documents.reshape(1, rows),
            out_weight,
            attn_gain.reshape(1, width),
            mlp_gain.reshape(1, width),
            wpack,
        )

    return local


def solution(mesh, ny=Y_DIM):
    blocks, tp = mesh.shape["sp"], mesh.shape["tp"]
    nz, nx = blocks // ny, tp // 2
    back = min((3 * blocks // 4 + ny - 1) // ny, nz - 1)
    placed = (
        P(("sp", "tp"), None),
        P("sp", "tp"),
        P("sp", "tp"),
        P("sp", "tp"),
        P("tp", None),
        P("sp"),
        P("tp", None),
        P(),
        P(),
        P("sp", "tp"),
        P("sp", "tp"),
        P("tp", "sp"),
    )
    return jax.shard_map(
        make_local(nz, ny, nx, back),
        mesh=mesh,
        in_specs=placed,
        out_specs=P(("sp", "tp"), None),
        check_vma=False,
    )
```

time: 111 us -> 99.1 us (0.89)
  the two profiles are of different devices: /device:TPU:8 before, /device:TPU:20 now
where the time goes in v2:
time: 99.1 us; the launch traced here: 98.8 us
  Pallas kernels  95.8 us (97%)
  local copies, waits for them, and re-layouts  1.57 us (2%)
  other arithmetic  1.44 us (1%)
    pallas_call x1, Pallas kernels, local(): pl.pallas_call(functools.partial(layer_kernel, nz, ny, nx, back), out_sha...  95.8 us

profile of v2, /device:TPU:20, one launch (start us, length us, event | category | flops | bytes accessed | tf_op | source)
XLA Modules:
  0.0 98.8 jit_solution(12485860256483162540)
XLA Ops:
  0.0 1.4 %pad_maximum_fusion.wpack = bf16[3,32,512]{2,1,0:T(8,128)(2,1)} fusion(bf16[1,32,512]{2,1,0:T(8,128)(2,1)} %bitcast.8, bf16[1,32,512]{2,1,0:T(8,128)(2,1)} %bitcast.9, bf16[1,32,512]{2,1,0:T(8,128)(2,1)} %bitcast.10), kind=kLoop, calls=%fused_computation | loop fusion | flops 98304 | bytes 196608 | tf_op jit(solution)/shard_map/stack | solution.py:686
  1.4 95.8 %shard_map.118 = bf16[32,2048]{1,0:T(8,128)(2,1)} custom-call(bf16[32,2048]{1,0:T(8,128)(2,1)} %resid.1, bf16[256,256]{1,0:T(8,128)(2,1)} %q.1, bf16[256,128]{1,0:T(8,128)(2,1)} %k.1, bf16[256,128]{1,0:T(8,128)(2,1)} %v.1, f32[2,16384]{1,0:T(2,128)} %gates.1, s32[1,256]{1,0:T(1,128)} %bitcast.13, bf16[256,2048]{1,0:T(8,128)(2,1)} %outw.1, ...), custom_call_target="tpu_custom_call" | custom-call | tf_op jit(solution)/shard_map/pallas_call | solution.py:724
  97.3 1.6 %copy.14 = bf16[32,2048]{1,0:T(8,128)(2,1)} copy(bf16[32,2048]{1,0:T(8,128)(2,1)} %shard_map.118) | data formatting | bytes 262144

commit v3 on v2

--- a/solution.py
+++ b/solution.py
@@ -80,16 +80,24 @@
     nx,
     back,
     resid,
+    q_in,
+    k_in,
+    v_in,
+    gates_in,
+    docs_in,
+    outw,
+    attn_gain_in,
+    mlp_gain_in,
+    gate_w,
+    up_w,
+    down_w,
+    out,
     q,
-    k,
     v,
     gates,
     docs,
-    outw,
     attn_gain,
     mlp_gain,
-    wpack,
-    out,
     qa,
     kf,
     vt,
@@ -138,6 +146,8 @@
     wf_rs,
     g_ss,
     g_rs,
+    s_ss,
+    s_rs,
     l_ss,
 ):
     sp, tp = lax.axis_index("sp"), lax.axis_index("tp")
@@ -145,7 +155,7 @@
     x, c = lax.div(tp, 2), lax.rem(tp, 2)
     rows = q.shape[0]
     own_rows, width = resid.shape
-    hidden = wpack.shape[2]
+    hidden = gate_w.shape[1]
     scale = 1.0 / math.sqrt(HD)
     scale2 = scale * math.log2(math.e)
     la = [min(lanes, hidden - 128) for lanes in A_LANES]
@@ -169,10 +179,28 @@
     for device in greet:
         pl.semaphore_signal(barrier, inc=1, device_id=device, device_id_type=MESH)
 
-    own_wo = pltpu.make_async_copy(outw, wo.at[tp], l_ss)
-    own_wo.start()
+    loads = {}
+
+    def load(name, src, dst):
+        loads[name] = pltpu.make_async_copy(src, dst, l_ss.at[len(loads)])
+        loads[name].start()
+
+    load("q", q_in, q)
+    load("docs", docs_in, docs)
+    load("v", v_in, v)
+    load("k", k_in, kf.at[z, :, 0:HD])
+    load("gate", gate_w, wall.at[c, 0, z, y])
+    load("up", up_w, wall.at[c, 1, z, y])
+    load("down", down_w, wall.at[c, 2, z, y])
+    load("gates", gates_in, gates)
+    load("resid", resid, rall.at[x])
+    load("wo", outw, wo.at[tp])
+    load("attn_gain", attn_gain_in, attn_gain)
+    load("mlp_gain", mlp_gain_in, mlp_gain)
 
     with phase("prep"):
+        loads["docs"].wait()
+        loads["q"].wait()
         row16 = lax.broadcasted_iota(jnp.int32, (AUG, rows), 0)
         doc16 = jnp.broadcast_to(docs[...], (AUG, rows))
         for h in range(2):
@@ -182,9 +210,11 @@
             one_hot = jnp.where((row16 < 3) & (doc16 == row16), 1.0, 0.0)
             pick = jnp.where((row16 >= 3 + 3 * h) & (row16 < 6 + 3 * h), 1.0, 0.0)
             qa[y, HD : HD + AUG, h * rows : (h + 1) * rows] = (one_hot + pick).astype(BF16)
-        kf[z, :, 0:HD] = k[...]
+        loads["v"].wait()
         vt[z, 0:HD, :] = v[...].astype(F32).T.astype(BF16)
         vt[z, HD : HD + AUG, :] = jnp.where(row16 == 0, doc16.astype(F32), 0.0).astype(BF16)
+        for name in ("k", "gate", "up", "down"):
+            loads[name].wait()
 
     with phase("barrier_wait"):
         pl.semaphore_wait(barrier, len(greet))
@@ -217,7 +247,7 @@
         along_y,
         [
             lambda i: qa.at[i, 0 : HD + AUG, 0:rows],
-            lambda i: qa.at[i, 0 : HD + AUG, rows : 2 * rows],
+            lambda i: qa.at[i, 0:HD, rows : 2 * rows],
         ],
         q_ss,
         q_rs,
@@ -269,7 +299,6 @@
         w_rs,
     )
 
-    wall[c, :, z, y] = wpack[...]
     k_ring.send(0, [0])
     q_ring.send(0, [0])
     a1.send(0)
@@ -278,17 +307,24 @@
     q_ring.send(0, [1])
 
     wo_forwards = []
-
-    def forward_wo(i, u):
+    wo_at = {i: [] for i in range(nx)}
+
+    def forward_wo(i, u, rel):
         piece = wo.at[2 * i + c, u * heads_half : (u + 1) * heads_half]
         at = len(wo_forwards)
+        wo_at[rel % nx].append(at)
         wo_forwards.append(remote(piece, piece, wf_ss.at[at], wf_rs.at[at], sibling))
 
-    own_wo.wait()
+    loads["resid"].wait()
+    copies_r = []
+    for d in range(1, nx):
+        sems = (x_ss.at[1, d - 1], x_rs.at[1, d - 1])
+        copies_r.append(remote(rall.at[x], rall.at[x], *sems, along_x(lax.rem(x + d, nx))))
+    loads["wo"].wait()
     if nx > 1:
         wo_ring.send(0)
     for u in range(2):
-        forward_wo(x, u)
+        forward_wo(x, u, 0)
     pending_wo = [(s, u) for s in range(nx // 2) for u in range(2)]
 
     def relay_wo(count):
@@ -298,8 +334,14 @@
                 wo_ring.wait(s, [u])
             if s < wo_ring.last:
                 wo_ring.send(s + 1, [u])
-            for i in wo_ring.arrived(s):
-                forward_wo(i, u)
+            rels = (-1 - s, 1 + s) if s < wo_ring.last else (nx // 2,)
+            for i, rel in zip(wo_ring.arrived(s), rels):
+                forward_wo(i, u, rel)
+
+    def second_head(i):
+        seen = qa[i, HD : HD + AUG, 0:rows].astype(F32)
+        pick = jnp.where((row16 >= 6) & (row16 < 9), 1.0, 0.0)
+        qa[i, HD : HD + AUG, rows : 2 * rows] = jnp.where(row16 < 3, seen, pick).astype(BF16)
 
     def zero_rows(i, _):
         qa[i, HD + AUG :, :] = jnp.zeros((qa.shape[1] - HD - AUG, 2 * rows), BF16)
@@ -342,16 +384,20 @@
                 if s < ring.last:
                     ring.send(s + 1, [sub])
 
+    loads["gates"].wait()
     key_terms(z)
     for s in range(max(nz, ny) // 2):
         step_on(k_ring, s, [0])
         step_on(q_ring, s, [0])
+        if s <= q_ring.last:
+            for i in q_ring.arrived(s):
+                second_head(i)
         step_on(a1, s, [0, 1, 2])
         step_on(b1, s, [0, 1, 2])
         if s == b1.last:
             b2.send(0)
         if s == a1.last:
-            a2.send(0)
+            a2.send(0, [0, 1])
         step_on(k_ring, s, [1])
         step_on(q_ring, s, [1])
         if s <= k_ring.last:
@@ -359,10 +405,19 @@
                 key_terms(i)
     for w in range(3):
         forward_b(z, w)
-        forward_a(y, w)
+        if w < 2:
+            forward_a(y, w)
 
     pending_b = [(s, w) for s in range(b2.last + 1) for w in range(3)]
-    pending_a = [(s, w) for s in range(a2.last + 1) for w in range(3)]
+    pending_a = [(s, w) for s in range(a2.last + 1) for w in range(2)]
+    late_a = [(s, 2) for s in range(a2.last + 1)]
+
+    def start_late():
+        a2.send(0, [2])
+        forward_a(y, 2)
+
+    def relay_late():
+        relay(a2, late_a, forward_a, 1)
 
     def relay(ring, pending, onward, count):
         for _ in range(min(count, len(pending))):
@@ -385,9 +440,8 @@
     count = z - first_block
 
     def query_block(step):
-        odd = lax.rem(step, 2)
-        turn = lax.div(step + 1, 2)
-        return lax.rem(y + half + jnp.where(odd == 1, -turn, turn) + ny, ny)
+        d = 1 - c if step % 2 else c
+        return lax.rem(y + (half - (step + 1) // 2) * (1 - 2 * d) + ny, ny)
 
     def fold(a, op):
         return op(a.reshape(rows // 8, 8, 2 * rows), axis=0)
@@ -419,9 +473,9 @@
         return lax.fori_loop(1, count + 1, more, top8)
 
     def attend(step, top8):
-        slot = lax.rem(step, 2)
+        slot = step % 2
         top = highest(top8)
-        ahead = query_block(step + 1)
+        ahead = query_block(min(step + 1, ny - 1))
         next8 = score(1 - slot, 0, z, ahead, True)
         sum8, probs = weigh(slot, 0, top)
         acc[...] = dot(vt[z, 0:HD, :], probs)
@@ -435,8 +489,8 @@
             return next8, sum8 + part8
 
         next8, sum8 = lax.fori_loop(1, count + 1, more, (next8, sum8))
-        row8 = lax.broadcasted_iota(jnp.int32, (8, 2 * rows), 0)
-        stats[...] = jnp.where(row8 == 0, top, jnp.sum(sum8, axis=0, keepdims=True))
+        row2 = lax.broadcasted_iota(jnp.int32, (2, 2 * rows), 0)
+        stats[...] = jnp.where(row2 == 0, top, jnp.sum(sum8, axis=0, keepdims=True))
         return next8
 
     def lanes(h):
@@ -471,8 +525,8 @@
         keep = jnp.exp2(top - new)
         take = jnp.exp2(other - new)
         total = stats[1:2, :] * keep + sin[d, j, 1:2, :] * take
-        row8 = lax.broadcasted_iota(jnp.int32, (8, 2 * rows), 0)
-        stats[...] = jnp.where(row8 == 0, new, total)
+        row2 = lax.broadcasted_iota(jnp.int32, (2, 2 * rows), 0)
+        stats[...] = jnp.where(row2 == 0, new, total)
         for h in range(2):
             at = lanes(h)
             with phase("o_wait"):
@@ -482,7 +536,7 @@
 
     def pass_on(step):
         j = half - (step + 1) // 2
-        d = c if step == 0 else 1 - step % 2
+        d = 1 - c if step % 2 else c
         to = along_y(lax.rem(y + 1 - 2 * d + ny, ny))
 
         def send(h):
@@ -496,66 +550,94 @@
             send(0)
             send(1)
 
-        if step == 0:
-            plain()
-        elif j < half - 1:
+        if j < half - (step % 2):
             add_arrived(d, j, send)
         else:
-            pl.when(c == d)(lambda: add_arrived(d, j, send))
-            pl.when(c != d)(plain)
+            plain()
 
     with phase("first_scores"):
         top8 = first_scores()
-    plan = {
-        0: (0, 0, 1),
-        1: (1, 1, 0),
-        2: (1, 1, 0),
-        3: (1, 1, 1),
-        4: (0, 1, 0),
-        5: (1, 1, 1),
-        6: (1, 0, 0),
-        7: (1, 1, 1),
-    }
+    plan = [(0, 1, 0), (1, 0, 0), (1, 1, 1), (1, 1, 0), (1, 0, 0), (1, 1, 1), (1, 0, 0), (1, 1, 1)]
     for step in range(ny):
         with phase("attend"):
             top8 = attend(step, top8)
         if step < ny - 1:
             pass_on(step)
+        if step == min(2, ny - 2):
+            start_late()
+        if step in (5, 7):
+            relay_late()
         count_b, count_a, count_wo = plan[step]
         relay_b(count_b)
         relay_a(count_a)
         relay_wo(count_wo)
-    relay_wo(len(pending_wo))
-    rall[x] = resid[...]
-    copies_r = []
-    for d in range(1, nx):
-        sems = (x_ss.at[1, d - 1], x_rs.at[1, d - 1])
-        copies_r.append(remote(rall.at[x], rall.at[x], *sems, along_x(lax.rem(x + d, nx))))
+    def final_stats(d):
+        with phase("o_wait"):
+            stat_copy(0, d, 0, sibling).wait_recv()
+
+    ways = [None, None]
+    top = stats[0:1, :]
     for d in range(2):
         if half > 1:
-            add_arrived(d, 0, lambda h: None)
+            final_stats(d)
         else:
-            pl.when(c == d)(functools.partial(add_arrived, d, 0, lambda h: None))
-    with phase("join"):
-        joined = acc[...] / stats[1:2, :]
-        for h in range(2):
-            part = joined[:, lanes(h)].T.astype(BF16).reshape(nx, 2, own_rows, HD)
+
+            @pl.when(c == d)
+            def _():
+                final_stats(d)
+
+            @pl.when(c != d)
+            def _():
+                sin[d, 0] = jnp.full((2, 2 * rows), FLOOR, F32)
+                oin[d, 0] = jnp.zeros((HD, 2 * rows), BF16)
+
+        ways[d] = sin[d, 0, 0:1, :]
+        top = jnp.maximum(top, ways[d])
+    shares = [jnp.exp2(w - top) for w in ways]
+    keep = jnp.exp2(stats[0:1, :] - top)
+    total = stats[1:2, :] * keep
+    for d in range(2):
+        total = total + shares[d] * sin[d, 0, 1:2, :]
+    keep = keep / total
+    shares = [share / total for share in shares]
+    got = []
+    for h in range(2):
+        at = lanes(h)
+        for d in range(2):
+            with phase("o_wait"):
+                wait = out_copy(0, d, 0, h, sibling).wait_recv
+                if half > 1:
+                    wait()
+                else:
+                    pl.when(c == d)(wait)
+        with phase("join"):
+            joined = acc[:, at] * keep[:, at]
+            for d in range(2):
+                joined = joined + oin[d, 0, :, at].astype(F32) * shares[d][:, at]
+            part = joined.T.astype(BF16).reshape(nx, 2, own_rows, HD)
+            cols = slice(h * HD, (h + 1) * HD)
             for core in range(2):
-                att[core, :, :, h * HD : (h + 1) * HD] = part[:, core]
-
-    got = []
-    for dx in range(nx):
-        for dc in range(2):
-            if dx + dc:
-                to = (sp, 2 * lax.rem(x + dx, nx) + jnp.where(dc == 1, 1 - c, c))
-                at = 2 * dx + dc - 1
-                core = to[1] - 2 * lax.div(to[1], 2)
-                copy = remote(att.at[core], attall.at[tp], g_ss.at[at], g_rs.at[at], to)
-                source = 2 * lax.rem(x - dx + nx, nx) + jnp.where(dc == 1, 1 - c, c)
-                got.append((copy, source, dx))
+                att[core, :, :, cols] = part[:, core]
+        for dx in range(nx):
+            for dc in range(2):
+                if dx + dc:
+                    core = 1 - c if dc else c
+                    to = (sp, 2 * lax.rem(x + dx, nx) + core)
+                    n = 2 * dx + dc - 1
+                    copy = remote(
+                        att.at[core, :, :, cols],
+                        attall.at[tp, :, :, cols],
+                        g_ss.at[n, h],
+                        g_rs.at[n, h],
+                        to,
+                    )
+                    source = 2 * lax.rem(x - dx + nx, nx) + core
+                    got.append((copy, source, dx, dc))
+        relay_b(1)
+        relay_a(h)
+    relay_wo(len(pending_wo))
     core_rows = nx * own_rows
     chunk = min(512, width)
-    relay_a(1)
 
     def project(first, block, source):
         for at in range(0, width, chunk):
@@ -567,20 +649,28 @@
 
     with phase("outproj"):
         project(True, att[c].reshape(core_rows, 2 * HD), tp)
-    with phase("fwo_wait"):
-        for copy in wo_forwards:
-            copy.wait()
-    got.sort(key=lambda g: min(g[2], nx - g[2]))
-    for n, (copy, source, _) in enumerate(got):
+    near = sorted(range(len(got) // 2), key=lambda n: (min(got[n][2], nx - got[n][2]), got[n][3]))
+    for n, block in enumerate(near):
+        copy, source, dx, dc = got[block]
         with phase("ag_wait"):
             copy.wait()
+            got[len(near) + block][0].wait()
+        if dc:
+            with phase("fwo_wait"):
+                for at in wo_at[-dx % nx]:
+                    wo_forwards[at].wait()
         with phase("outproj"):
             project(False, attall[source].reshape(core_rows, 2 * HD), source)
-        if n in (2, 4, 6):
+        if n in (0, 3):
+            relay_late()
+        if n in (1, 3, 4, 5):
             relay_b(1)
-            relay_a(1 if n > 2 else 0)
+        if n in (1, 3):
+            relay_a(1)
     for copy in copies_r:
         copy.wait()
+    loads["attn_gain"].wait()
+    loads["mlp_gain"].wait()
 
     def normalize(i, _):
         span = pl.ds(pl.multiple_of(i * own_rows, own_rows), own_rows)
@@ -617,17 +707,22 @@
 
     zs = max(1, chunk * nz // width)
 
-    def down_cols(n, _):
+    size = zs * width // nz
+    copies = []
+
+    def down_cols(n):
         sums = 0.0
         for j in range(2):
-            w = wall[j, 2, pl.ds(n * zs, zs)].reshape(zs * width // nz, hidden)
+            w = wall[j, 2, n * zs : (n + 1) * zs].reshape(size, hidden)
             sums += lax.dot_general(
                 hid[j], w, (((1,), (1,)), ((), ())), preferred_element_type=F32
             )
-        size = zs * width // nz
-        cols = pl.ds(pl.multiple_of(n * size, size), size)
+        cols = slice(n * size, (n + 1) * size)
         ps2[:, :, cols] = sums.astype(BF16).reshape(nx, own_rows, size)
-        return 0
+        for d in range(1, nx):
+            to = lax.rem(x + d, nx)
+            sems = (s_ss.at[n, d - 1], s_rs.at[n, d - 1])
+            copies.append(remote(ps2.at[to, :, cols], pr2.at[x, :, cols], *sems, along_x(to)))
 
     forwarded(0)
     with phase("ffn_gate"):
@@ -635,17 +730,12 @@
     forwarded(1)
     with phase("ffn_up"):
         lax.fori_loop(0, 2, up_core, 0)
+    while late_a:
+        relay_late()
     forwarded(2)
     with phase("ffn_down"):
-        lax.fori_loop(0, nz // zs, down_cols, 0)
-
-    def to_owners(send, recv, which):
-        copies = []
-        for d in range(1, nx):
-            to = lax.rem(x + d, nx)
-            sems = (x_ss.at[which, d - 1], x_rs.at[which, d - 1])
-            copies.append(remote(send.at[to], recv.at[x], *sems, along_x(to)))
-        return copies
+        for n in range(nz // zs):
+            down_cols(n)
 
     def summed(send, recv):
         sums = send[x].astype(F32)
@@ -654,7 +744,7 @@
         return sums
 
     with phase("rs2_wait"):
-        for copy in to_owners(ps2, pr2, 0):
+        for copy in copies:
             copy.wait()
     out[...] = (mid[x] + 0.5 * summed(ps2, pr2)).astype(BF16)
     for ring in (k_ring, q_ring, a1, b1, a2, b2, wo_ring):
@@ -683,19 +773,24 @@
         rows = queries.shape[0]
         own_rows, width = resid.shape
         w_rows, hidden = gate_weight.shape
-        wpack = jnp.stack([gate_weight, up_weight, down_weight.T])
         dma = pltpu.SemaphoreType.DMA
         x_block = pltpu.VMEM((nx, own_rows, width), BF16)
         kz, ky = nz // 2, ny // 2
         scratch = [
+            pltpu.VMEM(queries.shape, BF16),
+            pltpu.VMEM(values.shape, BF16),
+            pltpu.VMEM(log_gates.shape, F32),
+            pltpu.VMEM((1, rows), jnp.int32),
+            pltpu.VMEM((1, width), F32),
+            pltpu.VMEM((1, width), F32),
             pltpu.VMEM((ny, 2 * HD, 2 * rows), BF16),
             pltpu.VMEM((nz, rows, 2 * HD), BF16),
             pltpu.VMEM((nz, HD + AUG, rows), BF16),
             pltpu.VMEM((ny - 1, HD, 2 * rows), BF16),
             pltpu.VMEM((2, ky, HD, 2 * rows), BF16),
-            pltpu.VMEM((ny - 1, 8, 2 * rows), F32),
-            pltpu.VMEM((2, ky, 8, 2 * rows), F32),
-            pltpu.VMEM((8, 2 * rows), F32),
+            pltpu.VMEM((ny - 1, 2, 2 * rows), F32),
+            pltpu.VMEM((2, ky, 2, 2 * rows), F32),
+            pltpu.VMEM((2, 2 * rows), F32),
             pltpu.VMEM((2, back + 1, rows, 2 * rows), F32),
             pltpu.VMEM((HD, 2 * rows), F32),
             pltpu.VMEM((2, nx, own_rows, 2 * HD), BF16),
@@ -718,13 +813,14 @@
         scratch += [dma((2, max(nx - 1, 1)))] * 2
         scratch += [dma((2, max(nx // 2, 1), 2))] * 2
         scratch += [dma((2 * nx,))] * 2
-        scratch += [dma((2 * nx,))] * 2
-        scratch += [dma]
+        scratch += [dma((2 * nx, 2))] * 2
+        scratch += [dma((max(1, width // 512), max(nx - 1, 1)))] * 2
+        scratch += [dma((12,))]
         vmem = pl.BlockSpec(memory_space=pltpu.VMEM)
         return pl.pallas_call(
             functools.partial(layer_kernel, nz, ny, nx, back),
             out_shape=jax.ShapeDtypeStruct((own_rows, width), BF16),
-            in_specs=[vmem] * 6 + [pl.BlockSpec(memory_space=pl.ANY)] + [vmem] * 3,
+            in_specs=[pl.BlockSpec(memory_space=pl.ANY)] * 12,
             out_specs=vmem,
             scratch_shapes=scratch,
             compiler_params=pltpu.CompilerParams(
@@ -740,7 +836,9 @@
             out_weight,
             attn_gain.reshape(1, width),
             mlp_gain.reshape(1, width),
-            wpack,
+            gate_weight,
+            up_weight,
+            down_weight.T,
         )
 
     return local

time: 99.1 us -> 87.6 us (0.88)
  the two profiles are of different devices: /device:TPU:20 before, /device:TPU:8 now
where the time goes in v3:
time: 87.6 us; the launch traced here: 87.5 us
  Pallas kernels  85.9 us (98%)
  local copies, waits for them, and re-layouts  1.57 us (2%)
    pallas_call x1, Pallas kernels, local(): pl.pallas_call(functools.partial(layer_kernel, nz, ny, nx, back), out_sha...  85.9 us

profile of v3, /device:TPU:8, one launch (start us, length us, event | category | flops | bytes accessed | tf_op | source)
XLA Modules:
  0.0 87.5 jit_solution(3209651455605160290)
XLA Ops:
  0.0 85.9 %shard_map.118 = bf16[32,2048]{1,0:T(8,128)(2,1)} custom-call(bf16[32,2048]{1,0:T(8,128)(2,1)} %resid.1, bf16[256,256]{1,0:T(8,128)(2,1)} %q_in.1, bf16[256,128]{1,0:T(8,128)(2,1)} %k_in.1, bf16[256,128]{1,0:T(8,128)(2,1)} %v_in.1, f32[2,16384]{1,0:T(2,128)} %gates_in.1, s32[1,256]{1,0:T(1,128)} %bitcast.7, bf16[256,2048]{1,0:T(8,128)(2,1)} %outw.1, ...), custom_call_target="tpu_custom_call" | custom-call | tf_op jit(solution)/shard_map/pallas_call | solution.py:820
  85.9 1.6 %copy.14 = bf16[32,2048]{1,0:T(8,128)(2,1)} copy(bf16[32,2048]{1,0:T(8,128)(2,1)} %shard_map.118) | data formatting | bytes 262144

commit v4 on v3

--- a/solution.py
+++ b/solution.py
@@ -389,9 +389,6 @@
     for s in range(max(nz, ny) // 2):
         step_on(k_ring, s, [0])
         step_on(q_ring, s, [0])
-        if s <= q_ring.last:
-            for i in q_ring.arrived(s):
-                second_head(i)
         step_on(a1, s, [0, 1, 2])
         step_on(b1, s, [0, 1, 2])
         if s == b1.last:
@@ -400,6 +397,9 @@
             a2.send(0, [0, 1])
         step_on(k_ring, s, [1])
         step_on(q_ring, s, [1])
+        if s <= q_ring.last:
+            for i in q_ring.arrived(s):
+                second_head(i)
         if s <= k_ring.last:
             for i in k_ring.arrived(s):
                 key_terms(i)
@@ -737,22 +737,21 @@
         for n in range(nz // zs):
             down_cols(n)
 
-    def summed(send, recv):
-        sums = send[x].astype(F32)
-        for d in range(1, nx):
-            sums = sums + recv[lax.rem(x + d, nx)].astype(F32)
-        return sums
-
-    with phase("rs2_wait"):
-        for copy in copies:
-            copy.wait()
-    out[...] = (mid[x] + 0.5 * summed(ps2, pr2)).astype(BF16)
     for ring in (k_ring, q_ring, a1, b1, a2, b2, wo_ring):
         ring.finish()
     for step in range(ny - 1):
         stat_copy(step, 0, 0, sibling).wait_send()
         for h in range(2):
             out_copy(step, 0, 0, h, sibling).wait_send()
+    for n in range(nz // zs):
+        with phase("rs2_wait"):
+            for copy in copies[n * (nx - 1) : (n + 1) * (nx - 1)]:
+                copy.wait()
+        cols = slice(n * size, (n + 1) * size)
+        sums = ps2[x, :, cols].astype(F32)
+        for d in range(1, nx):
+            sums = sums + pr2[lax.rem(x + d, nx), :, cols].astype(F32)
+        out[:, cols] = (mid[x, :, cols] + 0.5 * sums).astype(BF16)
 
 
 def make_local(nz, ny, nx, back):
@@ -819,7 +818,7 @@
         vmem = pl.BlockSpec(memory_space=pltpu.VMEM)
         return pl.pallas_call(
             functools.partial(layer_kernel, nz, ny, nx, back),
-            out_shape=jax.ShapeDtypeStruct((own_rows, width), BF16),
+            out_shape=pltpu.VMEM((own_rows, width), BF16),
             in_specs=[pl.BlockSpec(memory_space=pl.ANY)] * 12,
             out_specs=vmem,
             scratch_shapes=scratch,

time: 87.6 us -> 85.8 us (0.979)
  local copies, waits for them, and re-layouts: 1.57 us -> 0.66 us
  Pallas kernels: 85.9 us -> 85 us
    pallas_call x1, Pallas kernels: 85.9 us -> 85 us  [local(): pl.pallas_call(functools.partial(layer_kernel, nz, ny, nx, back), out_sha...]
    unnamed x1, local copies, waits for them, and re-layouts: 1.57 us -> 0.66 us
where the time goes in v4:
time: 85.8 us; the launch traced here: 85.6 us
  Pallas kernels  85 us (99%)
    pallas_call x1, Pallas kernels, local(): pl.pallas_call(functools.partial(layer_kernel, nz, ny, nx, back), out_sha...  85 us

profile of v4, /device:TPU:8, one launch (start us, length us, event | category | flops | bytes accessed | tf_op | source)
XLA Modules:
  0.0 85.6 jit_solution(12922569710247476511)
XLA Ops:
  0.0 85.0 %shard_map.118 = bf16[32,2048]{1,0:T(8,128)(2,1)S(1)} custom-call(bf16[32,2048]{1,0:T(8,128)(2,1)} %resid.1, bf16[256,256]{1,0:T(8,128)(2,1)} %q_in.1, bf16[256,128]{1,0:T(8,128)(2,1)} %k_in.1, bf16[256,128]{1,0:T(8,128)(2,1)} %v_in.1, f32[2,16384]{1,0:T(2,128)} %gates_in.1, s32[1,256]{1,0:T(1,128)} %bitcast.7, bf16[256,2048]{1,0:T(8,128)(2,1)} %outw.1, ...), custom_call_target="tpu_custom_call" | custom-call | tf_op jit(solution)/shard_map/pallas_call | solution.py:819
  85.0 0.7 copy.14
